TPU v7x, 32 devices: a whole 2x2x4 slice. The times are simulated.
32 devices in a mesh: sp: 8 (over z, y), tp: 4 (over x, core).
Axes of the slice: x: 2, y: 2, z: 4, core: 2. Of those that a mesh axis runs over, the one named last changes fastest.
Arguments:
- residual_in: bfloat16 [6144, 2048], P('sp', 'tp'), may hold values from -11 to 11
- queries: bfloat16 [6144, 1024], P('sp', 'tp'), may hold values from -6 to 6
- keys: bfloat16 [6144, 256], P('sp'), may hold values from -6 to 6
- values: bfloat16 [6144, 256], P('sp'), may hold values from -6 to 6
- query_gain: float32 [128], replicated, may hold values from 1.5 to 5
- key_norm_gain: float32 [128], replicated, may hold values from 1.5 to 5
- out_weight: bfloat16 [1024, 2048], P('tp'), may hold values from -0.1875 to 0.1875
- mlp_gain: float32 [2048], replicated, may hold values from 0.1 to 1.9
- gate_weight: bfloat16 [2048, 5632], P('sp', 'tp'), may hold values from -0.125 to 0.125
- up_weight: bfloat16 [2048, 5632], P('sp', 'tp'), may hold values from -0.125 to 0.125
- down_weight: bfloat16 [5632, 2048], P('tp', 'sp'), may hold values from -0.15625 to 0.15625
Outputs:
- layer_out: bfloat16 [6144, 2048], P('sp', 'tp')
All inputs are finite; a program needn't handle non-finite values.
Results may differ from a plain program's by a relative error of at most 0.012.
The roundings to bfloat16 on the way count: a program that leaves them out, or rounds other values in their place, can miss the bound.
Values may be sent and summed in bfloat16 or wider, within the bound.
A program may use at most 64 MiB of HBM per device.

v0:
```python
import functools
import jax
import jax.numpy as jnp
from jax import lax
from jax.experimental import pallas as pl
from jax.experimental.pallas import tpu as pltpu
from jax.sharding import PartitionSpec as P

D = 2048
HEAD_SIZE = 128
QUERY_HEADS = 8
KEY_VALUE_HEADS = 2
GRID = 64

eps = 1e-06
rotary_base = 10000.0
MESH = pl.DeviceIdType.MESH
VMEM_LIMIT = 60 * 1024 * 1024
F32 = jnp.float32
BF16 = jnp.bfloat16


def apply_rotary(vectors, grid_positions):
    half_size = vectors.shape[-1] // 2
    frequency = rotary_base ** (-jnp.arange(0, half_size, 2, dtype=F32) / half_size)
    grid_row = (grid_positions // GRID).astype(F32)
    grid_col = (grid_positions % GRID).astype(F32)
    angles = jnp.concatenate(
        [grid_row[:, None] * frequency, grid_col[:, None] * frequency], axis=-1
    )[:, None, :]
    cosine_table = jnp.cos(angles)
    sine_table = jnp.sin(angles)
    first_half = vectors[..., :half_size]
    second_half = vectors[..., half_size:]
    return jnp.concatenate(
        [
            first_half * cosine_table - second_half * sine_table,
            first_half * sine_table + second_half * cosine_table,
        ],
        axis=-1,
    )


def per_head_norm(vectors, gain):
    return vectors * lax.rsqrt(jnp.mean(vectors * vectors, axis=-1, keepdims=True) + eps) * gain


def remote(src, dst, send, recv, sp, tp):
    copy = pltpu.make_async_remote_copy(
        src_ref=src, dst_ref=dst, send_sem=send, recv_sem=recv,
        device_id={"sp": sp, "tp": tp}, device_id_type=MESH,
    )
    copy.start()
    return copy


def greet(peers):
    barrier = pltpu.get_barrier_semaphore()
    for sp, tp in peers:
        pl.semaphore_signal(
            barrier, inc=1, device_id={"sp": sp, "tp": tp}, device_id_type=MESH
        )
    pl.semaphore_wait(barrier, len(peers))


def place():
    sp = lax.axis_index("sp")
    tp = lax.axis_index("tp")
    return sp, tp, sp // 2, lax.rem(sp, 2), tp // 2, lax.rem(tp, 2)


def gather_kernel(nz, kv_ref, out_ref, sz, rz, sy, ry, sc, rc):
    sp, tp, z, y, x, c = place()
    rows = kv_ref.shape[0]
    half = rows // 2
    other = x * 2 + (1 - c)
    z_peers = [lax.rem(z + k, nz) * 2 + y for k in range(1, nz)]
    y_peer = z * 2 + 1 - y
    greet([(p, tp) for p in z_peers] + [(y_peer, tp), (sp, other)])

    def spot(owner):
        return out_ref.at[pl.ds(pl.multiple_of(owner * rows + c * half, half), half), :]

    own = kv_ref.at[pl.ds(pl.multiple_of(c * half, half), half), :]
    sends = []
    to_z = [
        remote(own, spot(sp), sz.at[k - 1], rz.at[k - 1], z_peers[k - 1], tp)
        for k in range(1, nz)
    ]
    to_y = [remote(own, spot(sp), sy.at[0], ry.at[0], y_peer, tp)]
    out_ref[pl.ds(pl.multiple_of(sp * rows, rows), rows), :] = kv_ref[...]
    to_core = []
    for k in range(1, nz):
        to_z[k - 1].wait_recv()
        block = spot(lax.rem(z - k + nz, nz) * 2 + y)
        to_y.append(remote(block, block, sy.at[k], ry.at[k], y_peer, tp))
        to_core.append(remote(block, block, sc.at[k - 1], rc.at[k - 1], sp, other))
    for k in range(nz):
        to_y[k].wait_recv()
        block = spot(lax.rem(z - k + nz, nz) * 2 + 1 - y)
        slot = nz - 1 + k
        to_core.append(remote(block, block, sc.at[slot], rc.at[slot], sp, other))
    for copy in to_core:
        copy.wait_recv()
    for copy in to_z + to_y + to_core:
        copy.wait_send()


def gather_keys(kv, n_sp):
    nz = n_sp // 2
    dma = pltpu.SemaphoreType.DMA
    return pl.pallas_call(
        functools.partial(gather_kernel, nz),
        out_shape=jax.ShapeDtypeStruct((n_sp * kv.shape[0], kv.shape[1]), kv.dtype),
        in_specs=[pl.BlockSpec(memory_space=pltpu.VMEM)],
        out_specs=pl.BlockSpec(memory_space=pltpu.VMEM),
        scratch_shapes=[dma((nz - 1,)), dma((nz - 1,)), dma((nz,)), dma((nz,)),
                        dma((2 * nz - 1,)), dma((2 * nz - 1,))],
        compiler_params=pltpu.CompilerParams(collective_id=0, has_side_effects=True),
        name="gather_keys",
    )(kv)


def attend_kernel(width, q_ref, kv_ref, o_ref):
    rows = q_ref.shape[0]
    factor = HEAD_SIZE ** (-0.5) * 1.4426950408889634
    q = q_ref[...]

    def step(i, state):
        top, total, acc = state
        at = pl.ds(pl.multiple_of(i * width, width), width)
        s = lax.dot_general(
            q, kv_ref[at, 0:HEAD_SIZE], (((1,), (1,)), ((), ())), preferred_element_type=F32
        )
        new_top = jnp.maximum(top, jnp.max(s, axis=1, keepdims=True))
        fade = jnp.exp2((top - new_top) * factor)
        w = jnp.exp2((s - new_top) * factor)
        total = total * fade + jnp.sum(w, axis=1, keepdims=True)
        acc = acc * fade + jnp.dot(
            w.astype(BF16), kv_ref[at, HEAD_SIZE:], preferred_element_type=F32
        )
        return new_top, total, acc

    start = (
        jnp.full((rows, 1), -1e30, F32), jnp.zeros((rows, 1), F32),
        jnp.zeros((rows, HEAD_SIZE), F32),
    )
    top, total, acc = lax.fori_loop(0, kv_ref.shape[0] // width, step, start, unroll=2)
    o_ref[...] = (acc / total).astype(BF16)


def attend(queries, kv):
    rows, columns = queries.shape
    heads = columns // HEAD_SIZE
    block = 256
    width = 1024
    keys = kv.shape[0]
    work = rows * heads * keys
    return pl.pallas_call(
        functools.partial(attend_kernel, width),
        out_shape=jax.ShapeDtypeStruct((rows, columns), BF16),
        grid=(heads, rows // block),
        in_specs=[
            pl.BlockSpec((block, HEAD_SIZE), lambda h, i: (i, h)),
            pl.BlockSpec((keys, kv.shape[1]), lambda h, i: (0, 0)),
        ],
        out_specs=pl.BlockSpec((block, HEAD_SIZE), lambda h, i: (i, h)),
        compiler_params=pltpu.CompilerParams(vmem_limit_bytes=VMEM_LIMIT),
        cost_estimate=pl.CostEstimate(
            flops=work * HEAD_SIZE * 4, bytes_accessed=keys * 512, transcendentals=work
        ),
        name="attend",
    )(queries, kv)


def norm_kernel(nx, proj_ref, res_ref, gain_ref, mid_ref, out_ref,
                from_core, outgo, from_x, squares, blocks, s1, r1, s2, r2, s3, r3, s4, r4, s5, r5):
    sp, tp, z, y, x, c = place()
    rows, own = res_ref.shape
    n_tp = 2 * nx
    other = x * 2 + 1 - c
    y_peer = z * 2 + 1 - y
    xs = [lax.rem(x + j, nx) for j in range(nx)]
    back = [lax.rem(x - j + nx, nx) for j in range(nx)]
    row_peers = [(sp, xs[j] * 2 + c) for j in range(1, nx)]
    cross = [(y_peer, xs[j] * 2 + c) for j in range(nx)]
    across = [(sp, xs[j] * 2 + 1 - c) for j in range(1, nx)]
    greet([(sp, other)] + row_peers + cross + across)

    def cols(t):
        return pl.ds(pl.multiple_of(t * own, own), own)

    step = rows // 8
    to_core = [
        remote(proj_ref.at[:, cols(xs[j] * 2 + 1 - c)], from_core.at[j],
               s1.at[j], r1.at[j], sp, other)
        for j in list(range(1, nx)) + [0]
    ]
    to_core = [to_core[-1]] + to_core[:-1]
    to_x = []
    for j in range(1, nx):
        to_core[j].wait_recv()

        @pl.loop(0, 8)
        def _(i):
            at = pl.ds(pl.multiple_of(i * step, step), step)
            outgo[j - 1, at, :] = (
                proj_ref[at, cols(xs[j] * 2 + c)].astype(F32) + from_core[j, at, :].astype(F32)
            ).astype(BF16)

        to_x.append(remote(outgo.at[j - 1], from_x.at[j - 1], s2.at[j - 1], r2.at[j - 1],
                           *row_peers[j - 1]))
    to_core[0].wait_recv()
    for copy in to_x:
        copy.wait_recv()
    ones = jnp.ones((8, own), F32)

    for i in range(rows // 256):
        at = pl.ds(i * 256, 256)
        total = proj_ref[at, cols(tp)].astype(F32) + from_core[0, at, :].astype(F32)
        for j in range(1, nx):
            total += from_x[j - 1, at, :].astype(F32)
        mid = res_ref[at, :].astype(F32) + total
        mid_ref[at, :] = mid
        squares[0, :, at] = lax.dot_general(
            ones, mid * mid, (((1,), (1,)), ((), ())),
            precision=lax.Precision.HIGHEST, preferred_element_type=F32,
        )
    peers = [(sp, other)] + row_peers + across
    sq = [
        remote(squares.at[0], squares.at[k + 1], s3.at[k], r3.at[k], *peers[k])
        for k in range(len(peers))
    ]
    for copy in sq:
        copy.wait_recv()
    for i in range(rows // 256):
        at = pl.ds(i * 256, 256)
        square = squares[0, :, at]
        for k in range(len(peers)):
            square += squares[k + 1, :, at]
        scale = lax.rsqrt(square.T[:, 0:1] / (n_tp * own) + eps)
        block = (mid_ref[at, :] * scale * gain_ref[...]).astype(BF16)
        blocks[0, at, :] = block[:, : own // 2]
        blocks[1, at, :] = block[:, own // 2 :]

    half = own // 2

    def spot(yy, t):
        return (pl.ds(pl.multiple_of(yy * rows, rows), rows),
                pl.ds(pl.multiple_of(t * half, half), half))

    targets = cross + row_peers
    sources = [(1 - y, back[j] * 2 + c) for j in range(nx)]
    sources += [(y, back[j] * 2 + c) for j in range(1, nx)]
    mine = spot(y, tp)
    far = []
    for k in range(len(targets)):
        side = 1 - y if k < nx else y
        for i in range(2):
            at = (lax.rem(i + side, 2),) + mine
            far.append(remote(blocks.at[i], out_ref.at[at], s4.at[2 * k + i], r4.at[2 * k + i],
                              *targets[k]))
    near = []
    for i in range(2):
        at = (lax.rem(i + y, 2),) + mine
        near.append(remote(blocks.at[i], out_ref.at[at], s5.at[i], r5.at[i], sp, other))
        out_ref[at] = blocks[i]
    for k in range(len(targets)):
        for i in range(2):
            far[2 * k + i].wait_recv()
            at = (lax.rem(i + y, 2),) + spot(*sources[k])
            slot = 2 * k + 2 + i
            near.append(remote(out_ref.at[at], out_ref.at[at], s5.at[slot], r5.at[slot], sp, other))
    for copy in near:
        copy.wait_recv()
    for copy in to_core + to_x + sq + far + near:
        copy.wait_send()


def project_norm(proj, res, gain, n_tp):
    nx = n_tp // 2
    rows, own = res.shape
    dma = pltpu.SemaphoreType.DMA
    n = 2 * nx
    vm = pl.BlockSpec(memory_space=pltpu.VMEM)
    return pl.pallas_call(
        functools.partial(norm_kernel, nx),
        out_shape=(
            jax.ShapeDtypeStruct((rows, own), F32),
            jax.ShapeDtypeStruct((2, 2 * rows, n_tp * own // 2), BF16),
        ),
        in_specs=[vm] * 3,
        out_specs=(vm, vm),
        scratch_shapes=[
            pltpu.VMEM((nx, rows, own), BF16),
            pltpu.VMEM((nx - 1, rows, own), BF16),
            pltpu.VMEM((nx - 1, rows, own), BF16),
            pltpu.VMEM((n, 8, rows), F32),
            pltpu.VMEM((2, rows, own // 2), BF16),
            dma((nx,)), dma((nx,)), dma((nx - 1,)), dma((nx - 1,)),
            dma((n - 1,)), dma((n - 1,)), dma((2 * n - 2,)), dma((2 * n - 2,)),
            dma((2 * n,)), dma((2 * n,)),
        ],
        compiler_params=pltpu.CompilerParams(
            collective_id=1, has_side_effects=True, vmem_limit_bytes=VMEM_LIMIT
        ),
        name="project_norm",
    )(proj, res, gain)


def down_kernel(nx, terms_ref, mid_ref, out_ref, from_core, outgo, from_y, from_x, relay,
                last_x, last_y, s1, r1, s2, r2, s3, r3, s4, r4, s5, r5):
    sp, tp, z, y, x, c = place()
    rows, own = mid_ref.shape
    half = rows // 2
    top, low = pl.ds(0, half), pl.ds(half, half)
    other = x * 2 + 1 - c
    y_peer = (z * 2 + 1 - y, tp)
    xs = [lax.rem(x + j, nx) for j in range(nx)]
    x_peers = [(sp, xs[j] * 2 + c) for j in range(nx)]
    greet([(sp, other), y_peer] + x_peers[1:])
    every = [(1 - y, xs[j]) for j in range(nx)] + [(y, xs[j]) for j in range(1, nx)] + [(y, x)]
    order = list(range(1, 2 * nx - 1)) + [0, 2 * nx - 1]

    def cols(t):
        return pl.ds(pl.multiple_of(t * own, own), own)

    near = {}
    for k in order:
        yy, xx = every[k]
        near[k] = remote(
            terms_ref.at[pl.ds(pl.multiple_of(yy * rows, rows), rows), cols(xx * 2 + 1 - c)],
            from_core.at[k], s1.at[k], r1.at[k], sp, other)
    step = rows // 8
    to_y, to_x, again = {}, {}, []
    for k in order[:-1]:
        yy, xx = every[k]
        near[k].wait_recv()

        @pl.loop(0, 8)
        def _(i):
            at = pl.ds(pl.multiple_of(i * step, step), step)
            here = pl.ds(pl.multiple_of(yy * rows + i * step, step), step)
            outgo[k, at, :] = (
                terms_ref[here, cols(xx * 2 + c)].astype(F32) + from_core[k, at, :].astype(F32)
            ).astype(BF16)

        if k < nx:
            to_y[k] = remote(outgo.at[k, top], from_y.at[k], s2.at[k], r2.at[k], *y_peer)
        j = k if k < nx else k - nx + 1
        if j > 0:
            slot = 2 * (j - 1) + (1 if k < nx else 0)
            to_x[slot] = remote(outgo.at[k, low], from_x.at[slot], s3.at[slot], r3.at[slot],
                                *x_peers[j])
    for j in range(1, nx):
        to_y[j].wait_recv()

        @pl.loop(0, 4)
        def _(i):
            at = pl.ds(pl.multiple_of(i * step, step), step)
            relay[j, at, :] = (
                outgo[nx + j - 1, at, :].astype(F32) + from_y[j, at, :].astype(F32)
            ).astype(BF16)

        again.append(remote(relay.at[j], last_x.at[j - 1], s4.at[j - 1], r4.at[j - 1],
                            *x_peers[j]))
    for j in range(1, nx):
        to_x[2 * j - 1].wait_recv()

    @pl.loop(0, 4)
    def _(i):
        at = pl.ds(pl.multiple_of(i * step, step), step)
        here = pl.ds(pl.multiple_of(half + i * step, step), step)
        total = outgo[0, here, :].astype(F32)
        for j in range(1, nx):
            total += from_x[2 * j - 1, at, :].astype(F32)
        relay[0, at, :] = total.astype(BF16)

    again.append(remote(relay.at[0], last_y, s5.at[0], r5.at[0], *y_peer))
    near[2 * nx - 1].wait_recv()
    to_y[0].wait_recv()
    for j in range(1, nx):
        to_x[2 * j - 2].wait_recv()
    for copy in again:
        copy.wait_recv()

    @pl.loop(0, 4)
    def _(i):
        at = pl.ds(pl.multiple_of(i * step, step), step)
        for part in range(2):
            to = pl.ds(pl.multiple_of(part * half + i * step, step), step)
            here = pl.ds(pl.multiple_of(y * rows + part * half + i * step, step), step)
            total = terms_ref[here, cols(tp)].astype(F32)
            total += from_core[2 * nx - 1, to, :].astype(F32)
            total += (from_y[0, at, :] if part == 0 else last_y[at, :]).astype(F32)
            for j in range(1, nx):
                total += (last_x[j - 1, at, :] if part == 0
                          else from_x[2 * j - 2, at, :]).astype(F32)
            out_ref[to, :] = (mid_ref[to, :] + 0.5 * total).astype(BF16)

    for copy in list(near.values()) + list(to_y.values()) + list(to_x.values()) + again:
        copy.wait_send()


def down_sum(terms, mid, n_tp):
    nx = n_tp // 2
    rows, own = mid.shape
    dma = pltpu.SemaphoreType.DMA
    n = 2 * nx
    vm = pl.BlockSpec(memory_space=pltpu.VMEM)
    return pl.pallas_call(
        functools.partial(down_kernel, nx),
        out_shape=jax.ShapeDtypeStruct((rows, own), BF16),
        in_specs=[vm] * 2,
        out_specs=vm,
        scratch_shapes=[
            pltpu.VMEM((n, rows, own), BF16),
            pltpu.VMEM((n - 1, rows, own), BF16),
            pltpu.VMEM((nx, rows // 2, own), BF16),
            pltpu.VMEM((n - 2, rows // 2, own), BF16),
            pltpu.VMEM((nx, rows // 2, own), BF16),
            pltpu.VMEM((nx - 1, rows // 2, own), BF16),
            pltpu.VMEM((rows // 2, own), BF16),
            dma((n,)), dma((n,)), dma((nx,)), dma((nx,)), dma((n - 2,)), dma((n - 2,)),
            dma((nx - 1,)), dma((nx - 1,)), dma((1,)), dma((1,)),
        ],
        compiler_params=pltpu.CompilerParams(
            collective_id=2, has_side_effects=True, vmem_limit_bytes=VMEM_LIMIT
        ),
        name="down_sum",
    )(terms, mid)


def on_device(n_sp, n_tp, residual_in, queries, keys, values, query_gain, key_norm_gain,
              out_weight, mlp_gain, gate_weight, up_weight, down_weight):
    local_rows = residual_in.shape[0]
    local_heads = queries.shape[1] // HEAD_SIZE
    queries_per_group = QUERY_HEADS // KEY_VALUE_HEADS
    tp_index = lax.axis_index("tp")
    sp_index = lax.axis_index("sp")
    low = lax.rem(sp_index, 2)

    pairs = [(i, i ^ 1) for i in range(n_sp)]
    lanes = [[i for i in range(n_sp) if i % 2 == r] for r in range(2)]
    units = gate_weight.shape[1] // 2

    def halves(weight, axis):
        keep = lax.dynamic_slice_in_dim(weight, low * units, units, axis)
        give = lax.dynamic_slice_in_dim(weight, (1 - low) * units, units, axis)
        return keep, give

    gate_keep, gate_give = halves(gate_weight, 1)
    up_keep, up_give = halves(up_weight, 1)
    down_keep, down_give = halves(down_weight, 0)
    both_keep = jnp.concatenate([gate_keep, up_keep], axis=1)
    both_got = lax.ppermute(jnp.concatenate([gate_give, up_give], axis=1), "sp", pairs)
    down_got = lax.ppermute(down_give, "sp", pairs)

    def ordered(kept, got, axis):
        return jnp.where(
            low == 0,
            jnp.concatenate([kept, got], axis=axis),
            jnp.concatenate([got, kept], axis=axis),
        )

    both_first = lax.all_gather(
        both_keep, "sp", axis=0, axis_index_groups=lanes, tiled=True
    )
    grid_positions = sp_index * local_rows + jnp.arange(local_rows, dtype=jnp.int32)
    shared = tp_index * local_heads // queries_per_group
    own_keys = lax.dynamic_slice_in_dim(keys, shared * HEAD_SIZE, HEAD_SIZE, 1)
    own_values = lax.dynamic_slice_in_dim(values, shared * HEAD_SIZE, HEAD_SIZE, 1)
    key_matrix = apply_rotary(
        per_head_norm(own_keys.astype(F32)[:, None, :], key_norm_gain), grid_positions
    )[:, 0, :].astype(BF16)
    query_rows = apply_rotary(
        per_head_norm(queries.astype(F32).reshape(local_rows, local_heads, HEAD_SIZE), query_gain),
        grid_positions,
    ).astype(BF16).reshape(local_rows, local_heads * HEAD_SIZE)
    own_kv, query_rows, both_got, down_got = lax.optimization_barrier(
        (jnp.concatenate([key_matrix, own_values], axis=1), query_rows, both_got, down_got)
    )
    both_second = lax.all_gather(
        both_got, "sp", axis=0, axis_index_groups=lanes, tiled=True
    )
    down = lax.all_gather(
        ordered(down_keep, down_got, 1), "sp", axis=1, axis_index_groups=lanes, tiled=True
    )
    kv = gather_keys(own_kv, n_sp)
    attended = attend(query_rows, kv)
    projected = jnp.dot(attended, out_weight, preferred_element_type=F32).astype(BF16)
    own_width = residual_in.shape[1]
    gain_own = lax.dynamic_slice_in_dim(mlp_gain, tp_index * own_width, own_width, 0)[None, :]
    residual_mid, normed = project_norm(projected, residual_in, gain_own, n_tp)
    assert n_sp == 2 * n_tp
    gate_up = jnp.dot(normed[0], both_first, preferred_element_type=F32)
    gate_up += jnp.dot(normed[1], both_second, preferred_element_type=F32)
    hidden = (jax.nn.silu(gate_up[:, :units]) * gate_up[:, units:]).astype(BF16)
    down_terms = jnp.dot(hidden, down, preferred_element_type=F32).astype(BF16)
    return down_sum(down_terms, residual_mid, n_tp)


def solution(mesh):
    in_specs = (
        P("sp", "tp"),
        P("sp", "tp"),
        P("sp", None),
        P("sp", None),
        P(),
        P(),
        P("tp", None),
        P(),
        P("sp", "tp"),
        P("sp", "tp"),
        P("tp", "sp"),
    )
    out_specs = P("sp", "tp")
    return jax.shard_map(
        functools.partial(on_device, mesh.shape["sp"], mesh.shape["tp"]),
        mesh=mesh, in_specs=in_specs, out_specs=out_specs, check_vma=False,
    )
```

profile of v0, /device:TPU:24, one launch (start us, length us, event | category | flops | bytes accessed | tf_op | source)
XLA Modules:
  0.0 273.6 jit_solution(17227365561765870275)
XLA Ops:
  6.5 2.2 constant_dynamic-slice_fusion.1
  8.8 1.1 pad_maximum_fusion.1
  10.0 1.1 pad_maximum_fusion
  11.0 1.5 collective-permute-start
  12.6 0.8 constant_dynamic-slice_fusion
  13.3 0.5 collective-permute-start.1
  13.9 1.4 reshape.222
  15.3 0.2 fusion.8
  15.5 0.3 broadcast_multiply_fusion.1
  15.8 1.7 fusion.12
  17.4 0.9 multiply_reduce_fusion
  18.4 0.2 fusion.10
  18.6 1.0 multiply_multiply_fusion
  19.6 1.4 subtract_convert_fusion
  21.0 1.8 subtract_convert_fusion.1
  22.8 1.1 pad_maximum_fusion.5
  23.9 0.8 copy.18
  24.7 0.1 maximum_bitcast_fusion
  24.8 0.8 pad_maximum_fusion.3.kv_ref
  25.6 11.3 %collective-permute-done.1 = bf16[704,256]{1,0:T(8,128)(2,1)} collective-permute-done((bf16[704,256]{1,0:T(8,128)(2,1)}, bf16[704,256]{1,0:T(8,128)(2,1)}, u32[]{:S(2)}, u32[]{:S(2)}) %collective-permute-start.1) | collective-permute-done | bytes 360480 | tf_op jit(solution)/shard_map/ppermute | solution.py:457
  37.0 0.9 copy-done.2
  38.0 2.1 maximum_select_fusion
  40.1 1.3 dynamic_slice.32
  41.5 53.3 %gather_keys.1.kv_ref = bf16[6144,256]{1,0:T(8,128)(2,1)} custom-call(bf16[768,256]{1,0:T(8,128)(2,1)} %pad_maximum_fusion.3.kv_ref), custom_call_target="tpu_custom_call" | custom-call | tf_op jit(solution)/shard_map/gather_keys/pallas_call | solution.py:112
  94.8 23.6 %attend.1 = bf16[768,256]{1,0:T(8,128)(2,1)} custom-call(bf16[768,256]{1,0:T(8,128)(2,1)} %bitcast.25, bf16[6144,256]{1,0:T(8,128)(2,1)} %gather_keys.1.kv_ref), custom_call_target="tpu_custom_call" | custom-call | flops 4831838208 | bytes 3145728 | tf_op jit(solution)/shard_map/attend/pallas_call | solution.py:159
  118.5 3.6 %convolution_convert_fusion.1.proj_ref = bf16[768,2048]{1,0:T(8,128)(2,1)} fusion(bf16[768,256]{1,0:T(8,128)(2,1)} %attend.1, bf16[256,2048]{1,0:T(8,128)(2,1)S(1)} %copy-done), kind=kOutput, calls=%fused_computation.4 | convolution fusion | flops 806879232 | bytes 4587520 | tf_op jit(solution)/shard_map/dot_general | solution.py:491
  122.1 72.9 %project_norm.1 = (f32[768,512]{1,0:T(8,128)}, bf16[2,1536,1024]{2,1,0:T(8,128)(2,1)}) custom-call(bf16[768,2048]{1,0:T(8,128)(2,1)} %convolution_convert_fusion.1.proj_ref, bf16[768,512]{1,0:T(8,128)(2,1)} %res_ref.1, f32[1,512]{1,0:T(1,128)} %bitcast.26), custom_call_target="tpu_custom_call" | custom-call | tf_op jit(solution)/shard_map/project_norm/pallas_call | solution.py:286
  195.1 10.8 %fusion.2 = f32[1536,1408]{0,1:T(8,128)} fusion(bf16[1024,1408]{1,0:T(8,128)(2,1)} %all-gather.4.cloned.1.call-done, bf16[2,1536,1024]{2,1,0:T(8,128)(2,1)} %get-tuple-element.13), kind=kOutput, calls=%fused_computation.6 | convolution fusion | flops 4429185024 | bytes 14680064 | tf_op jit(solution)/shard_map/dot_general | solution.py:496
  205.9 13.3 %convolution_add_fusion = f32[1536,1408]{0,1:T(8,128)} fusion(f32[1536,1408]{0,1:T(8,128)} %fusion.2, bf16[1024,1408]{1,0:T(8,128)(2,1)} %all-gather.6.cloned.1.call-done, bf16[2,1536,1024]{2,1,0:T(8,128)(2,1)} %get-tuple-element.13), kind=kOutput, calls=%fused_computation | convolution fusion | flops 4431347712 | bytes 23330816 | tf_op jit(solution)/shard_map/dot_general | solution.py:497
  219.2 10.2 %convolution_convert_fusion.terms_ref = bf16[1536,2048]{1,0:T(8,128)(2,1)} fusion(bf16[704,2048]{1,0:T(8,128)(2,1)} %all-gather.8.cloned.1.call-done, f32[1536,1408]{0,1:T(8,128)} %convolution_add_fusion), kind=kOutput, calls=%fused_computation.1 | convolution fusion | flops 4438818816 | bytes 17825792 | tf_op jit(solution)/shard_map/dot_general | solution.py:499
  229.4 35.5 %down_sum.1 = bf16[768,512]{1,0:T(8,128)(2,1)} custom-call(bf16[1536,2048]{1,0:T(8,128)(2,1)} %convolution_convert_fusion.terms_ref, f32[768,512]{1,0:T(8,128)} %get-tuple-element.16.mid_ref), custom_call_target="tpu_custom_call" | custom-call | tf_op jit(solution)/shard_map/down_sum/pallas_call | solution.py:411
  265.0 2.1 copy.20
  (28 shorter events, 0.3 us)
Async XLA Ops:
  6.5 111.9 %copy-start = (bf16[256,2048]{1,0:T(8,128)(2,1)S(1)}, bf16[256,2048]{1,0:T(8,128)(2,1)}, u32[]{:S(2)}) copy-start(bf16[256,2048]{1,0:T(8,128)(2,1)} %param.17) | copy-start | bytes 3145732
  6.5 188.5 %all-gather.4.cloned.1.call-start = ((), (), s32[]{:S(2)}) async-start(), calls=%async_computation | async-start | bytes 3604480 | tf_op jit(solution)/shard_map/all_gather | solution.py:466
  6.5 6.0 %copy-start.1 = (bf16[1408,256]{1,0:T(8,128)(2,1)S(1)}, bf16[1408,256]{1,0:T(8,128)(2,1)}, u32[]{:S(2)}) copy-start(bf16[1408,256]{1,0:T(8,128)(2,1)} %param.21) | copy-start | bytes 2162692
  8.8 6.5 %copy-start.3 = (bf16[768,256]{1,0:T(8,128)(2,1)S(1)}, bf16[768,256]{1,0:T(8,128)(2,1)}, u32[]{:S(2)}) copy-start(bf16[768,256]{1,0:T(8,128)(2,1)} %param.13) | copy-start | bytes 1179652
  9.9 196.0 %all-gather.6.cloned.1.call-start = ((), (), s32[]{:S(2)}) async-start(), calls=%async_computation.1 | async-start | bytes 3604480 | tf_op jit(solution)/shard_map/all_gather | solution.py:483
  11.0 25.9 %collective-permute-start = (bf16[256,1408]{1,0:T(8,128)(2,1)}, bf16[256,1408]{1,0:T(8,128)(2,1)S(1)}, u32[]{:S(2)}, u32[]{:S(2)}) collective-permute-start(bf16[256,1408]{1,0:T(8,128)(2,1)} %pad_maximum_fusion), channel_id=1, source_target_pairs={{0,4},{4,0},{8,12},{12,8},{16,20},{20,16},{24,28},{28,24},{1,5},{5... | collective-permute-start | bytes 2162696 | tf_op jit(solution)/shard_map/ppermute | solution.py:456
  13.3 5.0 %copy-start.5 = (f32[128]{0:T(128)S(1)}, f32[128]{0:T(128)}, u32[]{:S(2)}) copy-start(f32[128]{0:T(128)} %param.16) | copy-start | bytes 1540
  13.3 23.6 %collective-permute-start.1 = (bf16[704,256]{1,0:T(8,128)(2,1)}, bf16[704,256]{1,0:T(8,128)(2,1)}, u32[]{:S(2)}, u32[]{:S(2)}) collective-permute-start(bf16[704,256]{1,0:T(8,128)(2,1)} %get-tuple-element.28), channel_id=1, source_target_pairs={{0,4},{4,0},{8,12},{12,8},{16,20},{20,16},{24,28},{28,24},{1,5},{5... | collective-permute-start | bytes 1081352 | tf_op jit(solution)/shard_map/ppermute | solution.py:457
  15.2 3.4 %copy-start.6 = (f32[128]{0:T(128)S(1)}, f32[128]{0:T(128)}, u32[]{:S(2)}) copy-start(f32[128]{0:T(128)} %param.15) | copy-start | bytes 1540
  19.6 5.1 %copy-start.4 = (bf16[768,256]{1,0:T(8,128)(2,1)S(1)}, bf16[768,256]{1,0:T(8,128)(2,1)}, u32[]{:S(2)}) copy-start(bf16[768,256]{1,0:T(8,128)(2,1)} %param.14) | copy-start | bytes 1179652
  37.0 0.9 copy-start.2
  37.9 181.3 %all-gather.8.cloned.1.call-start = ((), (), s32[]{:S(2)}) async-start(), calls=%async_computation.2 | async-start | bytes 3604480 | tf_op jit(solution)/shard_map/all_gather | solution.py:486
Sparse Core Ops, SparseCore 0:
  10.1 74.1 all-gather.3
  85.8 57.6 all-gather.5
  145.1 57.7 all-gather.7
where the time goes:
time: 274 us
  Pallas kernels  185 us (68%)
  matrix products  38 us (14%)
  other arithmetic  13.7 us (5%)
  between operations  13.3 us (5%)
  waiting for transfers between devices  11.4 us (4%)
  local copies, waits for them, and re-layouts  9.61 us (4%)
    pallas_call x1, Pallas kernels, project_norm(): pl.pallas_call(functools.partial(norm_kernel, nx), out_shape=(jax.ShapeDt...  72.9 us
    pallas_call x1, Pallas kernels, gather_keys(): pl.pallas_call(functools.partial(gather_kernel, nz), out_shape=jax.ShapeD...  53.3 us
    pallas_call x1, Pallas kernels, down_sum(): pl.pallas_call(functools.partial(down_kernel, nx), out_shape=jax.ShapeDty...  35.5 us
    pallas_call x1, Pallas kernels, attend(): pl.pallas_call(functools.partial(attend_kernel, width), out_shape=jax.Sha...  23.6 us
    dot_general x1, matrix products, on_device(): gate_up += jnp.dot(normed[1], both_second, preferred_element_type=F32)  13.3 us
    ppermute x1, waiting for transfers between devices, on_device(): down_got = lax.ppermute(down_give, 'sp', pairs)  11.3 us
    dot_general x1, matrix products, on_device(): gate_up = jnp.dot(normed[0], both_first, preferred_element_type=F32)  10.8 us
    dot_general x1, matrix products, on_device(): down_terms = jnp.dot(hidden, down, preferred_element_type=F32).astype(BF16)  10.2 us
  transfers between devices with their start and end apart: 5, of which 1 were waited for; matrix products, arithmetic and copies ran while one was open for 16% of the time, Pallas kernels for 55%

commit v1 on v0

v1 whole, which is shorter than its diff:
```python
import functools
import jax
import jax.numpy as jnp
from jax import lax
from jax.experimental import pallas as pl
from jax.experimental.pallas import tpu as pltpu
from jax.sharding import PartitionSpec as P

D = 2048
HEAD_SIZE = 128
QUERY_HEADS = 8
KEY_VALUE_HEADS = 2
GRID = 64

eps = 1e-06
rotary_base = 10000.0
MESH = pl.DeviceIdType.MESH
VMEM_LIMIT = 60 * 1024 * 1024
F32 = jnp.float32
BF16 = jnp.bfloat16


def apply_rotary(vectors, grid_positions):
    half_size = vectors.shape[-1] // 2
    frequency = rotary_base ** (-jnp.arange(0, half_size, 2, dtype=F32) / half_size)
    grid_row = (grid_positions // GRID).astype(F32)
    grid_col = (grid_positions % GRID).astype(F32)
    angles = jnp.concatenate(
        [grid_row[:, None] * frequency, grid_col[:, None] * frequency], axis=-1
    )[:, None, :]
    cosine_table = jnp.cos(angles)
    sine_table = jnp.sin(angles)
    first_half = vectors[..., :half_size]
    second_half = vectors[..., half_size:]
    return jnp.concatenate(
        [
            first_half * cosine_table - second_half * sine_table,
            first_half * sine_table + second_half * cosine_table,
        ],
        axis=-1,
    )


def per_head_norm(vectors, gain):
    return vectors * lax.rsqrt(jnp.mean(vectors * vectors, axis=-1, keepdims=True) + eps) * gain


def remote(src, dst, send, recv, sp, tp):
    copy = pltpu.make_async_remote_copy(
        src_ref=src, dst_ref=dst, send_sem=send, recv_sem=recv,
        device_id={"sp": sp, "tp": tp}, device_id_type=MESH,
    )
    copy.start()
    return copy


def greet(peers):
    barrier = pltpu.get_barrier_semaphore()
    for sp, tp in peers:
        pl.semaphore_signal(
            barrier, inc=1, device_id={"sp": sp, "tp": tp}, device_id_type=MESH
        )
    pl.semaphore_wait(barrier, len(peers))


def place():
    sp = lax.axis_index("sp")
    tp = lax.axis_index("tp")
    return sp, tp, sp // 2, lax.rem(sp, 2), tp // 2, lax.rem(tp, 2)


def rows_at(index, size):
    return pl.ds(pl.multiple_of(index * size, size), size)


def layer_kernel(nz, nx, heads, q_ref, kv_ref, w_ref, res_ref, gain_ref, gu_ref, dn_ref,
                 mid_ref, normed_ref, gu_out, dn_out,
                 kvs, vt, top_s, sum_s, acc_s, proj, from_core, outgo, from_x, squares, block,
                 s_z, r_z, s_y, r_y, s_c, r_c, s1, r1, s2, r2, s3, r3,
                 s_ax, r_ax, s_az, r_az, s_ar, r_ar, s_ac, r_ac,
                 s_gz, r_gz, s_gy, r_gy, s_dz, r_dz, s_dy, r_dy):
    sp, tp, z, y, x, c = place()
    rows, own = res_ref.shape
    n_tp = 2 * nx
    half = rows // 2
    tile = 256 if rows % 256 == 0 else rows
    tiles = rows // tile
    other = x * 2 + 1 - c
    u = lax.rem(z, 2)
    z_at = [lax.rem(z + k, nz) for k in range(nz)]
    z_from = [lax.rem(z - k + nz, nz) for k in range(nz)]
    xs = [lax.rem(x + j, nx) for j in range(nx)]
    back = [lax.rem(x - j + nx, nx) for j in range(nx)]
    y_peer = (z * 2 + 1 - y, tp)
    core_peer = (sp, other)
    z_pair = ((z + 1 - 2 * u) * 2 + y, tp)
    z_peers = [(z_at[k] * 2 + y, tp) for k in range(1, nz)]
    row_peers = [(sp, xs[j] * 2 + c) for j in range(1, nx)]
    across = [(sp, xs[j] * 2 + 1 - c) for j in range(1, nx)]
    greet(z_peers + [y_peer, core_peer] + row_peers + across)

    def spot(owner, side):
        return kvs.at[pl.ds(pl.multiple_of(owner * rows + side * half, half), half), :]

    sends = []

    def send(src, dst, out, arrive, slot, to):
        copy = remote(src, dst, out.at[slot], arrive.at[slot], *to)
        sends.append(copy)
        return copy

    mine = kv_ref.at[rows_at(c, half), :]
    kz = [None] + [send(mine, spot(sp, c), s_z, r_z, k - 1, z_peers[k - 1]) for k in range(1, nz)]
    ky = [send(mine, spot(sp, c), s_y, r_y, 0, y_peer)]
    gz = [None] + [
        send(gu_ref.at[lax.rem(z_at[k], 2)], gu_out.at[rows_at(sp, gu_ref.shape[1]), :],
             s_gz, r_gz, k - 1, z_peers[k - 1])
        for k in range(1, nz)
    ]
    kvs[rows_at(sp, rows), :] = kv_ref[...]
    depth = gu_ref.shape[1]
    wide = dn_ref.shape[2]
    gu_out[rows_at(sp, depth), :] = gu_ref[u]
    dn_out[:, rows_at(sp, wide)] = dn_ref[u]

    top_s[...] = jnp.full(top_s.shape, -1e30, F32)
    sum_s[...] = jnp.zeros(sum_s.shape, F32)
    acc_s[...] = jnp.zeros(acc_s.shape, F32)
    factor = HEAD_SIZE ** (-0.5) * 1.4426950408889634

    def attend(owner):
        at = rows_at(owner, rows)
        vt[...] = kvs[at, HEAD_SIZE:].astype(F32).T.astype(BF16)

        @pl.loop(0, tiles)
        def _(i):
            for h in range(heads):
                q = q_ref[rows_at(i, tile), h * HEAD_SIZE : (h + 1) * HEAD_SIZE]
                s = lax.dot_general(
                    kvs[at, 0:HEAD_SIZE], q, (((1,), (1,)), ((), ())), preferred_element_type=F32
                )
                n = i * heads + h
                top = top_s[n]
                new_top = jnp.maximum(top, jnp.max(s, axis=0, keepdims=True))
                fade = jnp.exp2((top - new_top) * factor)
                w = jnp.exp2((s - new_top) * factor)
                top_s[n] = new_top
                sum_s[n] = sum_s[n] * fade + jnp.sum(w, axis=0, keepdims=True)
                acc_s[n] = acc_s[n] * fade + jnp.dot(
                    vt[...], w.astype(BF16), preferred_element_type=F32
                )

    kc = {}

    def over(k, side):
        owner = z_from[k] * 2 + side
        slot = 2 * k + (0 if side is y else 1)
        return owner, slot

    def to_core(k, row, slot):
        block_at = spot(z_from[k] * 2 + row, c)
        kc[slot] = send(block_at, block_at, s_c, r_c, slot, core_peer)

    def near_arrived(k):
        kz[k].wait_recv()
        block_at = spot(z_from[k] * 2 + y, c)
        ky.append(send(block_at, block_at, s_y, r_y, k, y_peer))
        to_core(k, y, 2 * k - 1)

    def far_arrived(k):
        ky[k].wait_recv()
        to_core(k, 1 - y, 2 * k)

    def use(slot, owner):
        kc[slot].wait_recv()
        attend(owner)

    attend(sp)
    far_arrived(0)
    if nz > 1:
        near_arrived(1)
    use(0, z * 2 + 1 - y)
    for k in range(1, nz):
        if k + 1 < nz:
            near_arrived(k + 1)
        else:
            far_arrived(1)
        use(2 * k - 1, z_from[k] * 2 + y)
    gy = [send(gu_ref.at[u], gu_out.at[rows_at(sp, depth), :], s_gy, r_gy, 0, y_peer)]
    for k in range(1, nz):
        if k + 1 < nz:
            far_arrived(k + 1)
        use(2 * k, z_from[k] * 2 + 1 - y)

    def cols(t):
        return rows_at(t, own)

    @pl.loop(0, tiles)
    def _(i):
        parts = [
            (acc_s[i * heads + h] / sum_s[i * heads + h]).astype(BF16) for h in range(heads)
        ]
        got = jnp.concatenate(parts, axis=0) if heads > 1 else parts[0]
        proj[rows_at(i, tile), :] = lax.dot_general(
            got, w_ref[...], (((0,), (0,)), ((), ())), preferred_element_type=F32
        ).astype(BF16)

    step = rows // 8
    near = [
        send(proj.at[:, cols(xs[j] * 2 + 1 - c)], from_core.at[j], s1, r1, j, core_peer)
        for j in list(range(1, nx)) + [0]
    ]
    near = [near[-1]] + near[:-1]
    to_x = []
    for j in range(1, nx):
        near[j].wait_recv()

        @pl.loop(0, 8)
        def _(i):
            at = rows_at(i, step)
            outgo[j - 1, at, :] = (
                proj[at, cols(xs[j] * 2 + c)].astype(F32) + from_core[j, at, :].astype(F32)
            ).astype(BF16)

        to_x.append(send(outgo.at[j - 1], from_x.at[j - 1], s2, r2, j - 1, row_peers[j - 1]))
    near[0].wait_recv()

    def relay_gu(k):
        gz[k].wait_recv()
        at = gu_out.at[rows_at(z_from[k] * 2 + y, depth), :]
        gy.append(send(at, at, s_gy, r_gy, k, y_peer))

    for copy in to_x:
        copy.wait_recv()
    ones = jnp.ones((8, own), F32)

    for i in range(tiles):
        at = pl.ds(i * tile, tile)
        total = proj[at, cols(tp)].astype(F32) + from_core[0, at, :].astype(F32)
        for j in range(1, nx):
            total += from_x[j - 1, at, :].astype(F32)
        mid = res_ref[at, :].astype(F32) + total
        mid_ref[at, :] = mid
        squares[0, :, at] = lax.dot_general(
            ones, mid * mid, (((1,), (1,)), ((), ())),
            precision=lax.Precision.HIGHEST, preferred_element_type=F32,
        )
    peers = [core_peer] + row_peers + across
    sq = [send(squares.at[0], squares.at[k + 1], s3, r3, k, peers[k]) for k in range(len(peers))]
    for copy in sq:
        copy.wait_recv()

    def home(uu, t):
        return normed_ref.at[rows_at(uu, rows), cols(t)]

    for i in range(tiles):
        at = pl.ds(i * tile, tile)
        square = squares[0, :, at]
        for k in range(len(peers)):
            square += squares[k + 1, :, at]
        scale = lax.rsqrt(square.T[:, 0:1] / (n_tp * own) + eps)
        block[at, :] = (mid_ref[at, :] * scale * gain_ref[...]).astype(BF16)
    az = send(block, home(u, tp), s_az, r_az, 0, z_pair)
    ax = [send(block, home(u, tp), s_ax, r_ax, j - 1, row_peers[j - 1]) for j in range(1, nx)]
    ac = [send(block, home(u, tp), s_ac, r_ac, 0, core_peer)]
    normed_ref[rows_at(u, rows), cols(tp)] = block[...]
    dz = [None] + [
        send(dn_ref.at[lax.rem(z_at[k], 2)], dn_out.at[:, rows_at(sp, wide)],
             s_dz, r_dz, k - 1, z_peers[k - 1])
        for k in range(1, nz)
    ]

    def on_core(uu, t, slot):
        at = home(uu, t)
        ac.append(send(at, at, s_ac, r_ac, slot, core_peer))

    relay_gu(1)
    for j in range(1, nx):
        ax[j - 1].wait_recv()
        on_core(u, back[j] * 2 + c, j)
    az.wait_recv()
    there = home(1 - u, tp)
    ar = [send(there, there, s_ar, r_ar, j - 1, row_peers[j - 1]) for j in range(1, nx)]
    on_core(1 - u, tp, nx)
    for k in range(2, nz):
        relay_gu(k)
    dy = [send(dn_ref.at[u], dn_out.at[:, rows_at(sp, wide)], s_dy, r_dy, 0, y_peer)]
    for j in range(1, nx):
        ar[j - 1].wait_recv()
        on_core(1 - u, back[j] * 2 + c, nx + j)
    for k in range(1, nz):
        dz[k].wait_recv()
        at = dn_out.at[:, rows_at(z_from[k] * 2 + y, wide)]
        dy.append(send(at, at, s_dy, r_dy, k, y_peer))
    for copy in ac + gy + dy:
        copy.wait_recv()
    for copy in sends:
        copy.wait_send()


def layer(q, kv, w, res, gain, gu, dn, n_sp, n_tp):
    nz, nx = n_sp // 2, n_tp // 2
    rows, own = res.shape
    heads = q.shape[1] // HEAD_SIZE
    tile = 256 if rows % 256 == 0 else rows
    count = heads * (rows // tile)
    width = n_tp * own
    dma = pltpu.SemaphoreType.DMA
    n = 2 * nx
    vm = pl.BlockSpec(memory_space=pltpu.VMEM)

    def two(k):
        return [dma((k,)), dma((k,))]

    return pl.pallas_call(
        functools.partial(layer_kernel, nz, nx, heads),
        out_shape=(
            jax.ShapeDtypeStruct((rows, own), F32),
            jax.ShapeDtypeStruct((2 * rows, width), BF16),
            jax.ShapeDtypeStruct((n_sp * gu.shape[1], gu.shape[2]), BF16),
            jax.ShapeDtypeStruct((dn.shape[1], n_sp * dn.shape[2]), BF16),
        ),
        in_specs=[vm] * 7,
        out_specs=(vm,) * 4,
        scratch_shapes=[
            pltpu.VMEM((n_sp * rows, 2 * HEAD_SIZE), BF16),
            pltpu.VMEM((HEAD_SIZE, rows), BF16),
            pltpu.VMEM((count, 1, tile), F32),
            pltpu.VMEM((count, 1, tile), F32),
            pltpu.VMEM((count, HEAD_SIZE, tile), F32),
            pltpu.VMEM((rows, width), BF16),
            pltpu.VMEM((nx, rows, own), BF16),
            pltpu.VMEM((nx - 1, rows, own), BF16),
            pltpu.VMEM((nx - 1, rows, own), BF16),
            pltpu.VMEM((n, 8, rows), F32),
            pltpu.VMEM((rows, own), BF16),
        ] + two(nz - 1) + two(nz) + two(2 * nz - 1) + two(nx) + two(nx - 1) + two(n - 1)
        + two(nx - 1) + two(1) + two(nx - 1) + two(2 * nx)
        + two(nz - 1) + two(nz) + two(nz - 1) + two(nz),
        compiler_params=pltpu.CompilerParams(
            collective_id=0, has_side_effects=True, vmem_limit_bytes=VMEM_LIMIT
        ),
        name="layer",
    )(q, kv, w, res, gain, gu, dn)


def down_kernel(nx, terms_ref, mid_ref, out_ref, from_core, outgo, from_y, from_x, relay,
                last_x, last_y, s1, r1, s2, r2, s3, r3, s4, r4, s5, r5):
    sp, tp, z, row, x, c = place()
    rows, own = mid_ref.shape
    half = rows // 2
    top, low = pl.ds(0, half), pl.ds(half, half)
    other = x * 2 + 1 - c
    y = lax.rem(z, 2)
    y_peer = ((z + 1 - 2 * y) * 2 + row, tp)
    xs = [lax.rem(x + j, nx) for j in range(nx)]
    x_peers = [(sp, xs[j] * 2 + c) for j in range(nx)]
    greet([(sp, other), y_peer] + x_peers[1:])
    every = [(1 - y, xs[j]) for j in range(nx)] + [(y, xs[j]) for j in range(1, nx)] + [(y, x)]
    order = list(range(1, 2 * nx - 1)) + [0, 2 * nx - 1]

    def cols(t):
        return pl.ds(pl.multiple_of(t * own, own), own)

    near = {}
    for k in order:
        yy, xx = every[k]
        near[k] = remote(
            terms_ref.at[pl.ds(pl.multiple_of(yy * rows, rows), rows), cols(xx * 2 + 1 - c)],
            from_core.at[k], s1.at[k], r1.at[k], sp, other)
    step = rows // 8
    to_y, to_x, again = {}, {}, []
    for k in order[:-1]:
        yy, xx = every[k]
        near[k].wait_recv()

        @pl.loop(0, 8)
        def _(i):
            at = pl.ds(pl.multiple_of(i * step, step), step)
            here = pl.ds(pl.multiple_of(yy * rows + i * step, step), step)
            outgo[k, at, :] = (
                terms_ref[here, cols(xx * 2 + c)].astype(F32) + from_core[k, at, :].astype(F32)
            ).astype(BF16)

        if k < nx:
            to_y[k] = remote(outgo.at[k, top], from_y.at[k], s2.at[k], r2.at[k], *y_peer)
        j = k if k < nx else k - nx + 1
        if j > 0:
            slot = 2 * (j - 1) + (1 if k < nx else 0)
            to_x[slot] = remote(outgo.at[k, low], from_x.at[slot], s3.at[slot], r3.at[slot],
                                *x_peers[j])
    for j in range(1, nx):
        to_y[j].wait_recv()

        @pl.loop(0, 4)
        def _(i):
            at = pl.ds(pl.multiple_of(i * step, step), step)
            relay[j, at, :] = (
                outgo[nx + j - 1, at, :].astype(F32) + from_y[j, at, :].astype(F32)
            ).astype(BF16)

        again.append(remote(relay.at[j], last_x.at[j - 1], s4.at[j - 1], r4.at[j - 1],
                            *x_peers[j]))
    for j in range(1, nx):
        to_x[2 * j - 1].wait_recv()

    @pl.loop(0, 4)
    def _(i):
        at = pl.ds(pl.multiple_of(i * step, step), step)
        here = pl.ds(pl.multiple_of(half + i * step, step), step)
        total = outgo[0, here, :].astype(F32)
        for j in range(1, nx):
            total += from_x[2 * j - 1, at, :].astype(F32)
        relay[0, at, :] = total.astype(BF16)

    again.append(remote(relay.at[0], last_y, s5.at[0], r5.at[0], *y_peer))
    near[2 * nx - 1].wait_recv()
    to_y[0].wait_recv()
    for j in range(1, nx):
        to_x[2 * j - 2].wait_recv()
    for copy in again:
        copy.wait_recv()

    @pl.loop(0, 4)
    def _(i):
        at = pl.ds(pl.multiple_of(i * step, step), step)
        for part in range(2):
            to = pl.ds(pl.multiple_of(part * half + i * step, step), step)
            here = pl.ds(pl.multiple_of(y * rows + part * half + i * step, step), step)
            total = terms_ref[here, cols(tp)].astype(F32)
            total += from_core[2 * nx - 1, to, :].astype(F32)
            total += (from_y[0, at, :] if part == 0 else last_y[at, :]).astype(F32)
            for j in range(1, nx):
                total += (last_x[j - 1, at, :] if part == 0
                          else from_x[2 * j - 2, at, :]).astype(F32)
            out_ref[to, :] = (mid_ref[to, :] + 0.5 * total).astype(BF16)

    for copy in list(near.values()) + list(to_y.values()) + list(to_x.values()) + again:
        copy.wait_send()


def down_sum(terms, mid, n_tp):
    nx = n_tp // 2
    rows, own = mid.shape
    dma = pltpu.SemaphoreType.DMA
    n = 2 * nx
    vm = pl.BlockSpec(memory_space=pltpu.VMEM)
    return pl.pallas_call(
        functools.partial(down_kernel, nx),
        out_shape=jax.ShapeDtypeStruct((rows, own), BF16),
        in_specs=[vm] * 2,
        out_specs=vm,
        scratch_shapes=[
            pltpu.VMEM((n, rows, own), BF16),
            pltpu.VMEM((n - 1, rows, own), BF16),
            pltpu.VMEM((nx, rows // 2, own), BF16),
            pltpu.VMEM((n - 2, rows // 2, own), BF16),
            pltpu.VMEM((nx, rows // 2, own), BF16),
            pltpu.VMEM((nx - 1, rows // 2, own), BF16),
            pltpu.VMEM((rows // 2, own), BF16),
            dma((n,)), dma((n,)), dma((nx,)), dma((nx,)), dma((n - 2,)), dma((n - 2,)),
            dma((nx - 1,)), dma((nx - 1,)), dma((1,)), dma((1,)),
        ],
        compiler_params=pltpu.CompilerParams(
            collective_id=1, has_side_effects=True, vmem_limit_bytes=VMEM_LIMIT
        ),
        name="down_sum",
    )(terms, mid)


def on_device(n_sp, n_tp, residual_in, queries, keys, values, query_gain, key_norm_gain,
              out_weight, mlp_gain, gate_weight, up_weight, down_weight):
    local_rows = residual_in.shape[0]
    local_heads = queries.shape[1] // HEAD_SIZE
    queries_per_group = QUERY_HEADS // KEY_VALUE_HEADS
    tp_index = lax.axis_index("tp")
    sp_index = lax.axis_index("sp")
    units = gate_weight.shape[1] // 2
    gate_up = jnp.stack([
        jnp.concatenate(
            [w[:, part * units : (part + 1) * units] for w in (gate_weight, up_weight)], axis=1
        )
        for part in range(2)
    ])
    down = down_weight.reshape(2, units, down_weight.shape[1])

    grid_positions = sp_index * local_rows + jnp.arange(local_rows, dtype=jnp.int32)
    shared = tp_index * local_heads // queries_per_group
    own_keys = lax.dynamic_slice_in_dim(keys, shared * HEAD_SIZE, HEAD_SIZE, 1)
    own_values = lax.dynamic_slice_in_dim(values, shared * HEAD_SIZE, HEAD_SIZE, 1)
    key_matrix = apply_rotary(
        per_head_norm(own_keys.astype(F32)[:, None, :], key_norm_gain), grid_positions
    )[:, 0, :].astype(BF16)
    query_rows = apply_rotary(
        per_head_norm(queries.astype(F32).reshape(local_rows, local_heads, HEAD_SIZE), query_gain),
        grid_positions,
    ).astype(BF16).reshape(local_rows, local_heads * HEAD_SIZE)
    own_kv = jnp.concatenate([key_matrix, own_values], axis=1)
    own_width = residual_in.shape[1]
    gain_own = lax.dynamic_slice_in_dim(mlp_gain, tp_index * own_width, own_width, 0)[None, :]
    residual_mid, normed, gate_up, down = layer(
        query_rows, own_kv, out_weight, residual_in, gain_own, gate_up, down, n_sp, n_tp
    )
    gate_up = jnp.dot(normed, gate_up, preferred_element_type=F32)
    hidden = (jax.nn.silu(gate_up[:, :units]) * gate_up[:, units:]).astype(BF16)
    down_terms = jnp.dot(hidden, down, preferred_element_type=F32).astype(BF16)
    return down_sum(down_terms, residual_mid, n_tp)


def solution(mesh):
    in_specs = (
        P("sp", "tp"),
        P("sp", "tp"),
        P("sp", None),
        P("sp", None),
        P(),
        P(),
        P("tp", None),
        P(),
        P("sp", "tp"),
        P("sp", "tp"),
        P("tp", "sp"),
    )
    out_specs = P("sp", "tp")
    return jax.shard_map(
        functools.partial(on_device, mesh.shape["sp"], mesh.shape["tp"]),
        mesh=mesh, in_specs=in_specs, out_specs=out_specs, check_vma=False,
    )
```

time: 274 us -> 266 us (0.971)
  the two profiles are of different devices: /device:TPU:24 before, /device:TPU:0 now
where the time goes in v1:
time: 266 us
  Pallas kernels  225 us (85%)
  matrix products  21.4 us (8%)
  other arithmetic  13 us (5%)
  local copies, waits for them, and re-layouts  6.1 us (2%)
    pallas_call x1, Pallas kernels, layer(): pl.pallas_call(functools.partial(layer_kernel, nz, nx, heads), out_shape=...  191 us
    pallas_call x1, Pallas kernels, down_sum(): pl.pallas_call(functools.partial(down_kernel, nx), out_shape=jax.ShapeDty...  34.2 us
    dot_general x1, matrix products, on_device(): gate_up = jnp.dot(normed, gate_up, preferred_element_type=F32)  14.1 us
    dot_general x1, matrix products, on_device(): down_terms = jnp.dot(hidden, down, preferred_element_type=F32).astype(BF16)  7.29 us

profile of v1, /device:TPU:0, one launch (start us, length us, event | category | flops | bytes accessed | tf_op | source)
XLA Modules:
  0.0 265.9 jit_solution(1897460415449947424)
XLA Ops:
  0.0 0.0 copy-start
  0.0 0.0 copy-start.2
  0.1 1.5 dynamic_slice.11
  1.5 1.1 fusion.3
  2.7 0.0 copy-done
  2.7 1.1 fusion.5
  3.8 1.4 reshape.226
  5.2 0.9 multiply_reduce_fusion
  6.1 0.1 add_rsqrt_fusion
  6.2 0.0 copy-done.3
  6.2 1.0 multiply_multiply_fusion
  7.2 0.0 copy-done.1
  7.2 0.2 fusion.20
  7.3 0.0 copy-done.2
  7.4 0.2 fusion.21
  7.5 0.4 maximum_bitcast_fusion
  8.0 1.3 pad_maximum_fusion.gu_ref
  9.2 0.3 fusion.10
  9.5 1.8 subtract_convert_fusion.1
  11.3 0.1 maximum_bitcast_fusion.2
  11.4 0.8 pad_maximum_fusion.4.kv_ref
  12.3 1.6 fusion.9
  13.9 1.4 subtract_convert_fusion
  15.3 1.1 pad_maximum_fusion.2
  16.4 0.8 copy.18
  17.2 191.0 %layer.1 = (f32[768,512]{1,0:T(8,128)}, bf16[1536,2048]{1,0:T(8,128)(2,1)}, bf16[2048,1408]{1,0:T(8,128)(2,1)}, bf16[704,2048]{1,0:T(8,128)(2,1)}) custom-call(bf16[768,256]{1,0:T(8,128)(2,1)} %bitcast.21, bf16[768,256]{1,0:T(8,128)(2,1)} %pad_maximum_fusion.4.kv_ref, bf16[256,2048]{1,0:T(8,128)(2,1)} %w_ref.1, bf16[768,512]{1,0:T(8,128)(2,1)} %res_ref.1, ...), custom_call_target="tpu_custom_call" | custom-call | tf_op jit(solution)/shard_map/layer/pallas_call | solution.py:315
  208.2 0.0 copy-start.4
  208.2 14.1 %fusion.22 = f32[1536,1408]{0,1:T(8,128)S(1)} fusion(bf16[1536,2048]{1,0:T(8,128)(2,1)} %get-tuple-element.9, bf16[2048,1408]{1,0:T(8,128)(2,1)} %get-tuple-element.10), kind=kOutput, calls=%fused_computation.53 | convolution fusion | flops 8858370048 | bytes 20709376 | tf_op jit(solution)/shard_map/dot_general | solution.py:504
  222.3 0.0 copy-done.4
  222.3 7.3 %convolution_convert_fusion.terms_ref = bf16[1536,2048]{1,0:T(8,128)(2,1)} fusion(bf16[704,2048]{1,0:T(8,128)(2,1)S(1)} %copy-done.4, f32[1536,1408]{0,1:T(8,128)S(1)} %fusion.22), kind=kOutput, calls=%fused_computation | convolution fusion | flops 4438818816 | bytes 17825792 | tf_op jit(solution)/shard_map/dot_general | solution.py:506
  229.6 34.2 %down_sum.1 = bf16[768,512]{1,0:T(8,128)(2,1)} custom-call(bf16[1536,2048]{1,0:T(8,128)(2,1)} %convolution_convert_fusion.terms_ref, f32[768,512]{1,0:T(8,128)} %get-tuple-element.12.mid_ref), custom_call_target="tpu_custom_call" | custom-call | tf_op jit(solution)/shard_map/down_sum/pallas_call | solution.py:448
  263.8 2.1 copy.20
  (6 shorter events, 0.1 us)
Async XLA Ops:
  0.0 2.7 %copy-start = (bf16[768,256]{1,0:T(8,128)(2,1)S(1)}, bf16[768,256]{1,0:T(8,128)(2,1)}, u32[]{:S(2)}) copy-start(bf16[768,256]{1,0:T(8,128)(2,1)} %param.14) | copy-start | bytes 1179652
  0.0 7.3 %copy-start.2 = (bf16[256,1408]{1,0:T(8,128)(2,1)S(1)}, bf16[256,1408]{1,0:T(8,128)(2,1)}, u32[]{:S(2)}) copy-start(bf16[256,1408]{1,0:T(8,128)(2,1)} %param.20) | copy-start | bytes 2162692
  0.0 7.2 %copy-start.1 = (bf16[256,1408]{1,0:T(8,128)(2,1)S(1)}, bf16[256,1408]{1,0:T(8,128)(2,1)}, u32[]{:S(2)}) copy-start(bf16[256,1408]{1,0:T(8,128)(2,1)} %param.19) | copy-start | bytes 2162692
  0.0 6.2 %copy-start.3 = (f32[128]{0:T(128)S(1)}, f32[128]{0:T(128)}, u32[]{:S(2)}) copy-start(f32[128]{0:T(128)} %param.15) | copy-start | bytes 1540
  208.2 14.1 %copy-start.4 = (bf16[704,2048]{1,0:T(8,128)(2,1)S(1)}, bf16[704,2048]{1,0:T(8,128)(2,1)}, u32[]{:S(2)}) copy-start(bf16[704,2048]{1,0:T(8,128)(2,1)} %get-tuple-element.11) | copy-start | bytes 8650756

commit v2 on v1

v2 whole, which is shorter than its diff:
```python
import functools
import jax
import numpy as np
import jax.numpy as jnp
from jax import lax
from jax.experimental import pallas as pl
from jax.experimental.pallas import tpu as pltpu
from jax.sharding import PartitionSpec as P

D = 2048
HEAD_SIZE = 128
QUERY_HEADS = 8
KEY_VALUE_HEADS = 2
GRID = 64

eps = 1e-06
rotary_base = 10000.0
MESH = pl.DeviceIdType.MESH
VMEM_LIMIT = 67043328
F32 = jnp.float32
BF16 = jnp.bfloat16


def remote(src, dst, send, recv, sp, tp):
    copy = pltpu.make_async_remote_copy(
        src_ref=src, dst_ref=dst, send_sem=send, recv_sem=recv,
        device_id={"sp": sp, "tp": tp}, device_id_type=MESH,
    )
    copy.start()
    return copy


def greet(peers):
    barrier = pltpu.get_barrier_semaphore()
    for sp, tp in peers:
        pl.semaphore_signal(
            barrier, inc=1, device_id={"sp": sp, "tp": tp}, device_id_type=MESH
        )
    pl.semaphore_wait(barrier, len(peers))


def place():
    sp = lax.axis_index("sp")
    tp = lax.axis_index("tp")
    return sp, tp, sp // 2, lax.rem(sp, 2), tp // 2, lax.rem(tp, 2)


def rows_at(index, size):
    return pl.ds(pl.multiple_of(index * size, size), size)


def rotary_tables(tokens):
    half_size = HEAD_SIZE // 2
    frequency = np.float32(rotary_base) ** (
        -np.arange(0, half_size, 2, dtype=np.float32) / np.float32(half_size)
    )
    longest = max(tokens // GRID, GRID)
    angles = np.arange(longest, dtype=np.float32)[:, None] * frequency.astype(np.float32)
    cosine, sine = np.cos(angles), np.sin(angles)
    none = np.zeros_like(angles)
    rows = tokens // GRID
    pieces = [
        np.concatenate([cosine, none, cosine, none], axis=1)[:rows],
        np.concatenate([none, cosine, none, cosine], axis=1)[:GRID],
        np.concatenate([-sine, none, sine, none], axis=1)[:rows],
        np.concatenate([none, -sine, none, sine], axis=1)[:GRID],
    ]
    return [jnp.asarray(piece, F32) for piece in pieces]


def layer_kernel(nz, nx, heads, q_in, k_in, v_in, q_gain, k_gain, w_ref, res_ref, gain_ref,
                 gate_ref, up_ref, dn_ref, cos_row, cos_col, sin_row, sin_col,
                 out_ref,
                 q_ref, kv_ref, kvs, vt, top_s, sum_s, acc_s, proj, from_core, outgo, from_x,
                 squares, block, mid_ref, normed_ref, gu_ref, gu_all, dn_all, gu_acc, hidden,
                 terms, d_core, d_out, d_y, d_x, relay, last_x, last_y,
                 s_z, r_z, s_y, r_y, s_c, r_c, s1, r1, s2, r2, s3, r3,
                 s_ax, r_ax, s_az, r_az, s_ar, r_ar, s_ac, r_ac,
                 s_gz, r_gz, s_gy, r_gy, s_dz, r_dz, s_dy, r_dy,
                 e1, f1, e2, f2, e3, f3, e4, f4, e5, f5):
    sp, tp, z, y, x, c = place()
    rows, own = res_ref.shape
    n_tp = 2 * nx
    half = rows // 2
    tile = 256 if rows % 256 == 0 else rows
    tiles = rows // tile
    depth, twice = gate_ref.shape
    units = twice // 2
    wide = dn_ref.shape[2]
    other = x * 2 + 1 - c
    u = lax.rem(z, 2)
    z_at = [lax.rem(z + k, nz) for k in range(nz)]
    z_from = [lax.rem(z - k + nz, nz) for k in range(nz)]
    xs = [lax.rem(x + j, nx) for j in range(nx)]
    back = [lax.rem(x - j + nx, nx) for j in range(nx)]
    y_peer = (z * 2 + 1 - y, tp)
    core_peer = (sp, other)
    z_other = z + 1 - 2 * u
    z_pair = (z_other * 2 + y, tp)
    z_peers = [(z_at[k] * 2 + y, tp) for k in range(1, nz)]
    row_peers = [(sp, xs[j] * 2 + c) for j in range(1, nx)]
    across = [(sp, xs[j] * 2 + 1 - c) for j in range(1, nx)]

    def turn(ref, gain, columns, i):
        at = rows_at(i, GRID)
        v = ref[at, columns].astype(F32)
        v = v * lax.rsqrt(jnp.mean(v * v, axis=1, keepdims=True) + eps) * gain[...]
        row = sp * (rows // GRID) + i
        cosine = cos_row[pl.ds(row, 1), :] + cos_col[...]
        sine = sin_row[pl.ds(row, 1), :] + sin_col[...]
        return at, (v * cosine + pltpu.roll(v, HEAD_SIZE // 2, 1) * sine).astype(BF16)

    with jax.named_scope("prep"):
        shared = pl.ds(
            pl.multiple_of(tp * heads // (QUERY_HEADS // KEY_VALUE_HEADS) * HEAD_SIZE, HEAD_SIZE),
            HEAD_SIZE,
        )

        @pl.loop(0, rows // GRID)
        def _(i):
            at, turned = turn(k_in, k_gain, shared, i)
            kv_ref[at, 0:HEAD_SIZE] = turned
            kv_ref[at, HEAD_SIZE:] = v_in[at, shared]

        for part in range(2):
            cut = slice(part * units, (part + 1) * units)
            for i in range(0, depth, 64):
                gu_ref[part, i : i + 64, :] = jnp.concatenate(
                    [gate_ref[i : i + 64, cut].astype(F32), up_ref[i : i + 64, cut].astype(F32)],
                    axis=1,
                ).astype(BF16)

    with jax.named_scope("greet"):
        greet(z_peers + [y_peer, core_peer] + row_peers + across)

    def spot(owner, side):
        return kvs.at[pl.ds(pl.multiple_of(owner * rows + side * half, half), half), :]

    sends = []

    def send(src, dst, out, arrive, slot, to):
        copy = remote(src, dst, out.at[slot], arrive.at[slot], *to)
        sends.append(copy)
        return copy

    def got(name, copy):
        with jax.named_scope("w_" + name):
            copy.wait_recv()

    mine = kv_ref.at[rows_at(c, half), :]
    kz = [None] + [send(mine, spot(sp, c), s_z, r_z, k - 1, z_peers[k - 1]) for k in range(1, nz)]
    ky = [send(mine, spot(sp, c), s_y, r_y, 0, y_peer)]
    kvs[rows_at(sp, rows), :] = kv_ref[...]
    gu_all[rows_at(sp, depth), :] = gu_ref[u]
    dn_all[:, rows_at(sp, wide)] = dn_ref[u]

    with jax.named_scope("prep_q"):
        for h in range(heads):
            columns = slice(h * HEAD_SIZE, (h + 1) * HEAD_SIZE)

            @pl.loop(0, rows // GRID)
            def _(i):
                at, turned = turn(q_in, q_gain, columns, i)
                q_ref[at, columns] = turned

        top_s[...] = jnp.full(top_s.shape, -1e30, F32)
        sum_s[...] = jnp.zeros(sum_s.shape, F32)
        acc_s[...] = jnp.zeros(acc_s.shape, F32)
    factor = HEAD_SIZE ** (-0.5) * 1.4426950408889634

    def attend(owner):
        at = rows_at(owner, rows)
        with jax.named_scope("attend"):
            vt[...] = kvs[at, HEAD_SIZE:].astype(F32).T.astype(BF16)

            @pl.loop(0, tiles)
            def _(i):
                for h in range(heads):
                    q = q_ref[rows_at(i, tile), h * HEAD_SIZE : (h + 1) * HEAD_SIZE]
                    s = lax.dot_general(
                        kvs[at, 0:HEAD_SIZE], q, (((1,), (1,)), ((), ())),
                        preferred_element_type=F32,
                    )
                    n = i * heads + h
                    top = top_s[n]
                    new_top = jnp.maximum(top, jnp.max(s, axis=0, keepdims=True))
                    fade = jnp.exp2((top - new_top) * factor)
                    w = jnp.exp2((s - new_top) * factor)
                    top_s[n] = new_top
                    sum_s[n] = sum_s[n] * fade + jnp.sum(w, axis=0, keepdims=True)
                    acc_s[n] = acc_s[n] * fade + jnp.dot(
                        vt[...], w.astype(BF16), preferred_element_type=F32
                    )

    kc = {}

    def to_core(k, row, slot):
        at = spot(z_from[k] * 2 + row, c)
        kc[slot] = send(at, at, s_c, r_c, slot, core_peer)

    def near_arrived(k):
        got("kz", kz[k])
        at = spot(z_from[k] * 2 + y, c)
        ky.append(send(at, at, s_y, r_y, k, y_peer))
        to_core(k, y, 2 * k - 1)

    def far_arrived(k):
        got("ky", ky[k])
        to_core(k, 1 - y, 2 * k)

    def use(slot, owner):
        got("kc", kc[slot])
        attend(owner)

    order = [1] if nz == 2 else list(range(1, nz))
    attend(sp)
    far_arrived(0)
    near_arrived(1)
    use(0, z * 2 + 1 - y)
    gz, gy = {}, {}
    for k in range(1, nz):
        if k + 1 < nz:
            near_arrived(k + 1)
        else:
            far_arrived(1)
        if k + 1 == nz - 1 or nz == 2:
            with jax.named_scope("w_kzs"):
                for i in range(1, nz):
                    kz[i].wait_send()
            for i in order:
                gz[i] = send(gu_ref.at[lax.rem(z_at[i], 2)], gu_all.at[rows_at(sp, depth), :],
                             s_gz, r_gz, i - 1, z_peers[i - 1])
        use(2 * k - 1, z_from[k] * 2 + y)
    gy[0] = send(gu_ref.at[u], gu_all.at[rows_at(sp, depth), :], s_gy, r_gy, 0, y_peer)
    for k in range(1, nz):
        if k + 1 < nz:
            far_arrived(k + 1)
        use(2 * k, z_from[k] * 2 + 1 - y)

    def cols(t):
        return rows_at(t, own)

    with jax.named_scope("proj"):
        @pl.loop(0, tiles)
        def _(i):
            parts = [
                (acc_s[i * heads + h] / sum_s[i * heads + h]).astype(BF16) for h in range(heads)
            ]
            whole = jnp.concatenate(parts, axis=0) if heads > 1 else parts[0]
            proj[rows_at(i, tile), :] = lax.dot_general(
                whole, w_ref[...], (((0,), (0,)), ((), ())), preferred_element_type=F32
            ).astype(BF16)

    step = rows // 8
    near = [
        send(proj.at[:, cols(xs[j] * 2 + 1 - c)], from_core.at[j], s1, r1, j, core_peer)
        for j in list(range(1, nx)) + [0]
    ]
    near = [near[-1]] + near[:-1]
    to_x = []
    for j in range(1, nx):
        got("near", near[j])

        @pl.loop(0, 8)
        def _(i):
            at = rows_at(i, step)
            outgo[j - 1, at, :] = (
                proj[at, cols(xs[j] * 2 + c)].astype(F32) + from_core[j, at, :].astype(F32)
            ).astype(BF16)

        to_x.append(send(outgo.at[j - 1], from_x.at[j - 1], s2, r2, j - 1, row_peers[j - 1]))
    got("near0", near[0])

    def relay_gu(k):
        got("gz", gz[k])
        at = gu_all.at[rows_at(z_from[k] * 2 + y, depth), :]
        gy[k] = send(at, at, s_gy, r_gy, k, y_peer)

    relay_gu(order[0])
    dy = {0: send(dn_ref.at[u], dn_all.at[:, rows_at(sp, wide)], s_dy, r_dy, 0, y_peer)}

    for copy in to_x:
        got("tox", copy)
    ones = jnp.ones((8, own), F32)

    with jax.named_scope("mid"):
        for i in range(tiles):
            at = pl.ds(i * tile, tile)
            total = proj[at, cols(tp)].astype(F32) + from_core[0, at, :].astype(F32)
            for j in range(1, nx):
                total += from_x[j - 1, at, :].astype(F32)
            mid = res_ref[at, :].astype(F32) + total
            mid_ref[at, :] = mid
            squares[0, :, at] = lax.dot_general(
                ones, mid * mid, (((1,), (1,)), ((), ())),
                precision=lax.Precision.HIGHEST, preferred_element_type=F32,
            )
    peers = [core_peer] + row_peers + across
    sq = [send(squares.at[0], squares.at[k + 1], s3, r3, k, peers[k]) for k in range(len(peers))]
    for copy in sq:
        got("sq", copy)

    def home(uu, t):
        return normed_ref.at[rows_at(uu, rows), cols(t)]

    with jax.named_scope("norm"):
        for i in range(tiles):
            at = pl.ds(i * tile, tile)
            square = squares[0, :, at]
            for k in range(len(peers)):
                square += squares[k + 1, :, at]
            scale = lax.rsqrt(square.T[:, 0:1] / (n_tp * own) + eps)
            block[at, :] = (mid_ref[at, :] * scale * gain_ref[:, cols(tp)]).astype(BF16)
    az = send(block, home(u, tp), s_az, r_az, 0, z_pair)
    ax = [send(block, home(u, tp), s_ax, r_ax, j - 1, row_peers[j - 1]) for j in range(1, nx)]
    ac = [send(block, home(u, tp), s_ac, r_ac, 0, core_peer)]
    normed_ref[rows_at(u, rows), cols(tp)] = block[...]

    def on_core(uu, t, slot):
        at = home(uu, t)
        ac.append(send(at, at, s_ac, r_ac, slot, core_peer))

    for k in order[1:2]:
        relay_gu(k)
    for j in range(1, nx):
        got("ax", ax[j - 1])
        on_core(u, back[j] * 2 + c, j)
    got("az", az)
    there = home(1 - u, tp)
    ar = [send(there, there, s_ar, r_ar, j - 1, row_peers[j - 1]) for j in range(1, nx)]
    on_core(1 - u, tp, nx)
    dz = {
        k: send(dn_ref.at[lax.rem(z_at[k], 2)], dn_all.at[:, rows_at(sp, wide)],
                s_dz, r_dz, k - 1, z_peers[k - 1])
        for k in order
    }
    for k in order[2:]:
        relay_gu(k)

    def gate_up(owner, first=False):
        ks = rows_at(owner, depth)
        with jax.named_scope("gate_up"):
            @pl.loop(0, 2 * rows // 384)
            def _(i):
                at = rows_at(i, 384)
                term = jnp.dot(normed_ref[at, ks], gu_all[ks, :], preferred_element_type=F32)
                gu_acc[at, :] = term if first else gu_acc[at, :] + term

    def relay_dn(k):
        got("dz", dz[k])
        at = dn_all.at[:, rows_at(z_from[k] * 2 + y, wide)]
        dy[k] = send(at, at, s_dy, r_dy, k, y_peer)

    for j in range(1, nx):
        got("ar", ar[j - 1])
        on_core(1 - u, back[j] * 2 + c, nx + j)
    for copy in ac:
        got("ac", copy)
    gate_up(sp, True)
    for k in order:
        gate_up(z_from[k] * 2 + y)
    for k in [0] + order:
        got("gy", gy[k])
        gate_up(z_from[k] * 2 + 1 - y)
        if k > 0:
            relay_dn(k)

    with jax.named_scope("hidden"):
        @pl.loop(0, 2 * rows // 128)
        def _(i):
            at = rows_at(i, 128)
            gate = gu_acc[at, :units]
            hidden[at, :] = (gate / (1.0 + jnp.exp(-gate)) * gu_acc[at, units:]).astype(BF16)

    def down(owner):
        ks = rows_at(owner, wide)
        with jax.named_scope("down"):
            @pl.loop(0, 2 * rows // 384)
            def _(i):
                at = rows_at(i, 384)
                terms[at, ks] = jnp.dot(
                    hidden[at, :], dn_all[:, ks], preferred_element_type=F32
                ).astype(BF16)

    down(sp)
    for k in order:
        down(z_from[k] * 2 + y)
    for k in [0] + order:
        got("dy", dy[k])
        down(z_from[k] * 2 + 1 - y)

    top, low = pl.ds(0, half), pl.ds(half, half)
    x_peers = [(sp, xs[j] * 2 + c) for j in range(nx)]
    every = [(1 - u, xs[j]) for j in range(nx)] + [(u, xs[j]) for j in range(1, nx)] + [(u, x)]
    turns = list(range(1, 2 * nx - 1)) + [0, 2 * nx - 1]
    side = {}
    for k in turns:
        uu, xx = every[k]
        side[k] = send(terms.at[rows_at(uu, rows), cols(xx * 2 + 1 - c)], d_core.at[k],
                       e1, f1, k, core_peer)
    to_z, to_x, again = {}, {}, []
    for k in turns[:-1]:
        uu, xx = every[k]
        got("side", side[k])

        @pl.loop(0, 8)
        def _(i):
            at = rows_at(i, step)
            here = pl.ds(pl.multiple_of(uu * rows + i * step, step), step)
            d_out[k, at, :] = (
                terms[here, cols(xx * 2 + c)].astype(F32) + d_core[k, at, :].astype(F32)
            ).astype(BF16)

        if k < nx:
            to_z[k] = send(d_out.at[k, top], d_y.at[k], e2, f2, k, z_pair)
        j = k if k < nx else k - nx + 1
        if j > 0:
            slot = 2 * (j - 1) + (1 if k < nx else 0)
            to_x[slot] = send(d_out.at[k, low], d_x.at[slot], e3, f3, slot, x_peers[j])
    for j in range(1, nx):
        got("to_z", to_z[j])

        @pl.loop(0, 4)
        def _(i):
            at = rows_at(i, step)
            relay[j, at, :] = (
                d_out[nx + j - 1, at, :].astype(F32) + d_y[j, at, :].astype(F32)
            ).astype(BF16)

        again.append(send(relay.at[j], last_x.at[j - 1], e4, f4, j - 1, x_peers[j]))
    for j in range(1, nx):
        got("to_x", to_x[2 * j - 1])

    @pl.loop(0, 4)
    def _(i):
        at = rows_at(i, step)
        here = pl.ds(pl.multiple_of(half + i * step, step), step)
        total = d_out[0, here, :].astype(F32)
        for j in range(1, nx):
            total += d_x[2 * j - 1, at, :].astype(F32)
        relay[0, at, :] = total.astype(BF16)

    again.append(send(relay.at[0], last_y, e5, f5, 0, z_pair))
    got("side", side[2 * nx - 1])
    got("to_z", to_z[0])
    for j in range(1, nx):
        got("to_x", to_x[2 * j - 2])
    for copy in again:
        got("again", copy)

    with jax.named_scope("final"):
        @pl.loop(0, 4)
        def _(i):
            at = rows_at(i, step)
            for part in range(2):
                to = pl.ds(pl.multiple_of(part * half + i * step, step), step)
                here = pl.ds(pl.multiple_of(u * rows + part * half + i * step, step), step)
                total = terms[here, cols(tp)].astype(F32)
                total += d_core[2 * nx - 1, to, :].astype(F32)
                total += (d_y[0, at, :] if part == 0 else last_y[at, :]).astype(F32)
                for j in range(1, nx):
                    total += (last_x[j - 1, at, :] if part == 0
                              else d_x[2 * j - 2, at, :]).astype(F32)
                out_ref[to, :] = (mid_ref[to, :] + 0.5 * total).astype(BF16)

    kz_sends = {id(kz[i]) for i in range(1, nz)}
    with jax.named_scope("w_sends"):
        for copy in sends:
            if id(copy) not in kz_sends:
                copy.wait_send()


def layer(q, k, v, q_gain, k_gain, w, res, gain, gate, up, dn, n_sp, n_tp):
    nz, nx = n_sp // 2, n_tp // 2
    rows, own = res.shape
    heads = q.shape[1] // HEAD_SIZE
    tile = 256 if rows % 256 == 0 else rows
    count = heads * (rows // tile)
    width = n_tp * own
    depth, twice = gate.shape
    wide = dn.shape[2]
    dma = pltpu.SemaphoreType.DMA
    n = 2 * nx
    vm = pl.BlockSpec(memory_space=pltpu.VMEM)

    def two(k):
        return [dma((k,)), dma((k,))]

    def bf(*shape):
        return pltpu.VMEM(shape, BF16)

    def fl(*shape):
        return pltpu.VMEM(shape, F32)

    return pl.pallas_call(
        functools.partial(layer_kernel, nz, nx, heads),
        out_shape=jax.ShapeDtypeStruct((rows, own), BF16),
        in_specs=[vm] * 15,
        out_specs=vm,
        scratch_shapes=[
            bf(rows, heads * HEAD_SIZE), bf(rows, 2 * HEAD_SIZE),
            bf(n_sp * rows, 2 * HEAD_SIZE), bf(HEAD_SIZE, rows),
            fl(count, 1, tile), fl(count, 1, tile), fl(count, HEAD_SIZE, tile),
            bf(rows, width), bf(nx, rows, own), bf(nx - 1, rows, own), bf(nx - 1, rows, own),
            fl(n, 8, rows), bf(rows, own), fl(rows, own), bf(2 * rows, width),
            bf(2, depth, twice), bf(n_sp * depth, twice), bf(dn.shape[1], n_sp * wide),
            fl(2 * rows, twice), bf(2 * rows, twice // 2), bf(2 * rows, width),
            bf(n, rows, own), bf(n - 1, rows, own), bf(nx, rows // 2, own),
            bf(n - 2, rows // 2, own), bf(nx, rows // 2, own), bf(nx - 1, rows // 2, own),
            bf(rows // 2, own),
        ] + two(nz - 1) + two(nz) + two(2 * nz - 1) + two(nx) + two(nx - 1) + two(n - 1)
        + two(nx - 1) + two(1) + two(nx - 1) + two(2 * nx)
        + two(nz - 1) + two(nz) + two(nz - 1) + two(nz)
        + two(n) + two(nx) + two(n - 2) + two(nx - 1) + two(1),
        compiler_params=pltpu.CompilerParams(
            collective_id=0, has_side_effects=True, vmem_limit_bytes=VMEM_LIMIT
        ),
        name="layer",
    )(q, k, v, q_gain, k_gain, w, res, gain, gate, up, dn, *rotary_tables(n_sp * rows))


def on_device(n_sp, n_tp, residual_in, queries, keys, values, query_gain, key_norm_gain,
              out_weight, mlp_gain, gate_weight, up_weight, down_weight):
    down = down_weight.reshape(2, down_weight.shape[0] // 2, down_weight.shape[1])
    return layer(
        queries, keys, values, query_gain[None, :], key_norm_gain[None, :], out_weight,
        residual_in, mlp_gain[None, :], gate_weight, up_weight, down, n_sp, n_tp,
    )


def solution(mesh):
    in_specs = (
        P("sp", "tp"),
        P("sp", "tp"),
        P("sp", None),
        P("sp", None),
        P(),
        P(),
        P("tp", None),
        P(),
        P("sp", "tp"),
        P("sp", "tp"),
        P("tp", "sp"),
    )
    out_specs = P("sp", "tp")
    return jax.shard_map(
        functools.partial(on_device, mesh.shape["sp"], mesh.shape["tp"]),
        mesh=mesh, in_specs=in_specs, out_specs=out_specs, check_vma=False,
    )
```

time: 266 us -> 203 us (0.76)
  the two profiles are of different devices: /device:TPU:0 before, /device:TPU:16 now
where the time goes in v2:
time: 203 us
  Pallas kernels  201 us (99%)
  local copies, waits for them, and re-layouts  2.06 us (1%)
    pallas_call x1, Pallas kernels, layer(): pl.pallas_call(functools.partial(layer_kernel, nz, nx, heads), out_shape=...  201 us

profile of v2, /device:TPU:16, one launch (start us, length us, event | category | flops | bytes accessed | tf_op | source)
XLA Modules:
  0.0 202.9 jit_solution(1261198399165700723)
XLA Ops:
  0.0 200.8 %layer.1 = bf16[768,512]{1,0:T(8,128)(2,1)} custom-call(bf16[768,256]{1,0:T(8,128)(2,1)} %q_in.1, bf16[768,256]{1,0:T(8,128)(2,1)} %k_in.1, bf16[768,256]{1,0:T(8,128)(2,1)} %v_in.1, f32[1,128]{1,0:T(1,128)} %bitcast.6, f32[1,128]{1,0:T(1,128)} %bitcast.7, bf16[256,2048]{1,0:T(8,128)(2,1)} %w_ref.1, bf16[768,512]{1,0:T(8,128)(2,1)} %res_ref.1, ...), custom_call_target="tpu_custom_call" | custom-call | tf_op jit(solution)/shard_map/layer/pallas_call | solution.py:495
  200.8 2.1 %copy.17 = bf16[768,512]{1,0:T(8,128)(2,1)} copy(bf16[768,512]{1,0:T(8,128)(2,1)} %layer.1) | data formatting | bytes 1572864

commit v3 on v2

v3 whole, which is shorter than its diff:
```python
import functools
import jax
import numpy as np
import jax.numpy as jnp
from jax import lax
from jax.experimental import pallas as pl
from jax.experimental.pallas import tpu as pltpu
from jax.sharding import PartitionSpec as P

D = 2048
HEAD_SIZE = 128
QUERY_HEADS = 8
KEY_VALUE_HEADS = 2
GRID = 64

eps = 1e-06
rotary_base = 10000.0
MESH = pl.DeviceIdType.MESH
VMEM_LIMIT = 67043328
F32 = jnp.float32
BF16 = jnp.bfloat16


def remote(src, dst, send, recv, sp, tp):
    copy = pltpu.make_async_remote_copy(
        src_ref=src, dst_ref=dst, send_sem=send, recv_sem=recv,
        device_id={"sp": sp, "tp": tp}, device_id_type=MESH,
    )
    copy.start()
    return copy


def greet(peers):
    barrier = pltpu.get_barrier_semaphore()
    for sp, tp in peers:
        pl.semaphore_signal(
            barrier, inc=1, device_id={"sp": sp, "tp": tp}, device_id_type=MESH
        )
    pl.semaphore_wait(barrier, len(peers))


def place():
    sp = lax.axis_index("sp")
    tp = lax.axis_index("tp")
    return sp, tp, sp // 2, lax.rem(sp, 2), tp // 2, lax.rem(tp, 2)


def rows_at(index, size):
    return pl.ds(pl.multiple_of(index * size, size), size)


def rotary_tables(tokens):
    half_size = HEAD_SIZE // 2
    frequency = np.float32(rotary_base) ** (
        -np.arange(0, half_size, 2, dtype=np.float32) / np.float32(half_size)
    )
    longest = max(tokens // GRID, GRID)
    angles = np.arange(longest, dtype=np.float32)[:, None] * frequency.astype(np.float32)
    cosine, sine = np.cos(angles), np.sin(angles)
    none = np.zeros_like(angles)
    rows = tokens // GRID
    pieces = [
        np.concatenate([cosine, none, cosine, none], axis=1)[:rows],
        np.concatenate([none, cosine, none, cosine], axis=1)[:GRID],
        np.concatenate([-sine, none, sine, none], axis=1)[:rows],
        np.concatenate([none, -sine, none, sine], axis=1)[:GRID],
    ]
    return [jnp.asarray(piece, F32) for piece in pieces]


def layer_kernel(nz, nx, heads, q_in, k_in, v_in, q_gain, k_gain, w_ref, res_ref, gain_ref,
                 gate_ref, up_ref, dn_ref, cos_row, cos_col, sin_row, sin_col,
                 out_ref,
                 q_ref, kv_ref, kvs, vt, top_s, sum_s, acc_s, proj, from_core, outgo, from_x,
                 squares, block, mid_ref, normed_ref, gu_ref, gu_all, dn_all, gu_acc, hidden,
                 ratio, column, terms, d_core, d_out, d_y, d_x, relay, last_x, last_y,
                 s_z, r_z, s_f, s_y, r_y, s_c, r_c, s1, r1, s2, r2, s3, r3,
                 s_ax, r_ax, s_az, r_az, s_ar, r_ar, s_ac, r_ac,
                 s_rz, r_rz, s_gz, r_gz, s_gy, r_gy, s_dz, r_dz, s_dy, r_dy,
                 e1, f1, e2, f2, e3, f3, e4, f4, e5, f5):
    sp, tp, z, y, x, c = place()
    rows, own = res_ref.shape
    n_tp = 2 * nx
    half = rows // 2
    tile = 256 if rows % 256 == 0 else rows
    tiles = rows // tile
    depth, twice = gate_ref.shape
    units = twice // 2
    wide = dn_ref.shape[2]
    other = x * 2 + 1 - c
    u = lax.rem(z, 2)
    z_other = z + 1 - 2 * u
    nh = nz // 2
    inner = lax.rem(z // 2 + u, 2)
    flip = lax.rem(u + inner, 2)
    z_to, z_from, slots_z = [z_other], [z_other], [0]
    for d in range(1, nh):
        ahead = lax.rem(z // 2 + d, nh) * 2
        behind = lax.rem(z // 2 - d + nh, nh) * 2
        z_to += [ahead + flip, ahead + 1 - flip]
        z_from += [behind + flip, behind + 1 - flip]
        slots_z += [2 * d - 1 + inner, 2 * d - inner]
    xs = [lax.rem(x + j, nx) for j in range(nx)]
    back = [lax.rem(x - j + nx, nx) for j in range(nx)]
    y_peer = (z * 2 + 1 - y, tp)
    core_peer = (sp, other)
    z_pair = (z_other * 2 + y, tp)
    z_peers = [(k * 2 + y, tp) for k in z_to]
    far = range(nz - 1)
    row_peers = [(sp, xs[j] * 2 + c) for j in range(1, nx)]
    across = [(sp, xs[j] * 2 + 1 - c) for j in range(1, nx)]

    def turn(ref, gain, columns, i):
        at = rows_at(i, GRID)
        v = ref[at, columns].astype(F32)
        v = v * lax.rsqrt(jnp.mean(v * v, axis=1, keepdims=True) + eps) * gain[...]
        row = sp * (rows // GRID) + i
        cosine = cos_row[pl.ds(row, 1), :] + cos_col[...]
        sine = sin_row[pl.ds(row, 1), :] + sin_col[...]
        return at, (v * cosine + pltpu.roll(v, HEAD_SIZE // 2, 1) * sine).astype(BF16)

    barrier = pltpu.get_barrier_semaphore()
    friends = z_peers + [y_peer, core_peer] + row_peers + across
    for to_sp, to_tp in friends:
        pl.semaphore_signal(
            barrier, inc=1, device_id={"sp": to_sp, "tp": to_tp}, device_id_type=MESH
        )

    with jax.named_scope("prep"):
        shared = pl.ds(
            pl.multiple_of(tp * heads // (QUERY_HEADS // KEY_VALUE_HEADS) * HEAD_SIZE, HEAD_SIZE),
            HEAD_SIZE,
        )

        @pl.loop(0, rows // GRID, unroll=4)
        def _(i):
            at, turned = turn(k_in, k_gain, shared, i)
            kv_ref[at, 0:HEAD_SIZE] = turned
            kv_ref[at, HEAD_SIZE:] = v_in[at, shared]

        for part in range(2):
            cut = slice(part * units, (part + 1) * units)
            for i in range(0, depth, 64):
                gu_ref[part, i : i + 64, :] = jnp.concatenate(
                    [gate_ref[i : i + 64, cut].astype(F32), up_ref[i : i + 64, cut].astype(F32)],
                    axis=1,
                ).astype(BF16)

    with jax.named_scope("greet"):
        pl.semaphore_wait(barrier, len(friends))

    def spot(owner, side):
        return kvs.at[pl.ds(pl.multiple_of(owner * rows + side * half, half), half), :]

    sends = []

    def describe(src, dst, out, arrive, slot, to):
        copy = pltpu.make_async_remote_copy(
            src_ref=src, dst_ref=dst, send_sem=out.at[slot], recv_sem=arrive.at[slot],
            device_id={"sp": to[0], "tp": to[1]}, device_id_type=MESH,
        )
        sends.append(copy)
        return copy

    def send(src, dst, out, arrive, slot, to):
        copy = remote(src, dst, out.at[slot], arrive.at[slot], *to)
        sends.append(copy)
        return copy

    def got(name, copy):
        with jax.named_scope("w_" + name):
            copy.wait_recv()

    mine = kv_ref.at[rows_at(c, half), :]
    send(mine, spot(sp, c), s_z, r_z, 0, z_pair)
    key_from = [(z_other, 0)]
    for d in range(1, nh):
        ahead = lax.rem(z // 2 + d, nh)
        behind = lax.rem(z // 2 - d + nh, nh)
        target = ((ahead * 2 + lax.rem(ahead + 1, 2)) * 2 + y, tp)
        send(mine, spot(sp, c), s_z, r_z, 2 * d - 1 + u, target)
        key_from += [(behind * 2 + uu, 2 * d - 1 + uu) for uu in range(2)]
    passed = []
    ky = [send(mine, spot(sp, c), s_y, r_y, 0, y_peer)]
    gz, gy, dz, dy = {}, {}, {}, {}

    def pieces(k):
        return 1 if k <= 0 else 2

    def gu_at(owner, k, a):
        size = depth // pieces(k)
        return gu_all.at[pl.ds(pl.multiple_of(owner * depth + a * size, size), size), :]

    def give_gu(k):
        for a in range(pieces(k)):
            size = depth // pieces(k)
            gz[k, a] = describe(gu_ref.at[lax.rem(z_to[k], 2), pl.ds(a * size, size)],
                                gu_at(sp, k, a), s_gz, r_gz, slots_z[k] * 2 + a, z_peers[k])

    def give_dn(k):
        dz[k] = describe(dn_ref.at[lax.rem(z_to[k], 2)], dn_all.at[:, rows_at(sp, wide)],
                         s_dz, r_dz, slots_z[k], z_peers[k])

    dy[-1] = send(dn_ref.at[u], dn_all.at[:, rows_at(sp, wide)], s_dy, r_dy, 0, y_peer)
    for k in far:
        give_gu(k)
        give_dn(k)

    def give_pair():
        gz[0, 0].start()

    pl.when(inner == 0)(give_pair)
    dz[0].start()
    for k in far[1:]:
        for a in range(pieces(k)):
            gz[k, a].start()
    kvs[rows_at(sp, rows), :] = kv_ref[...]
    gu_all[rows_at(sp, depth), :] = gu_ref[u]
    dn_all[:, rows_at(sp, wide)] = dn_ref[u]

    with jax.named_scope("prep_q"):
        for h in range(heads):
            columns = slice(h * HEAD_SIZE, (h + 1) * HEAD_SIZE)

            @pl.loop(0, rows // GRID, unroll=4)
            def _(i):
                at, turned = turn(q_in, q_gain, columns, i)
                q_ref[at, columns] = turned

        top_s[...] = jnp.full(top_s.shape, -1e30, F32)
        sum_s[...] = jnp.zeros(sum_s.shape, F32)
        acc_s[...] = jnp.zeros(acc_s.shape, F32)
    factor = HEAD_SIZE ** (-0.5) * 1.4426950408889634

    def turn_values(owner):
        vt[owner] = kvs[rows_at(owner, rows), HEAD_SIZE:].astype(F32).T.astype(BF16)

    def attend(owner, start, stop):
        at = rows_at(owner, rows)
        with jax.named_scope("attend"):

            @pl.loop(start, stop)
            def _(i):
                slots = [i * heads + h for h in range(heads)]
                states = [(top_s[n], sum_s[n], acc_s[n]) for n in slots]
                scores = [
                    lax.dot_general(
                        kvs[at, 0:HEAD_SIZE],
                        q_ref[rows_at(i, tile), h * HEAD_SIZE : (h + 1) * HEAD_SIZE],
                        (((1,), (1,)), ((), ())), preferred_element_type=F32,
                    )
                    for h in range(heads)
                ]
                values = vt[owner]
                for n, s, (top, total, acc) in zip(slots, scores, states):
                    new_top = jnp.maximum(top, jnp.max(s, axis=0, keepdims=True))
                    fade = jnp.exp2((top - new_top) * factor)
                    w = jnp.exp2((s - new_top) * factor)
                    top_s[n] = new_top
                    sum_s[n] = total * fade + jnp.sum(w, axis=0, keepdims=True)
                    acc_s[n] = acc * fade + jnp.dot(
                        values, w.astype(BF16), preferred_element_type=F32
                    )

    kc = {}
    first = max(tiles - 1, 1)

    def to_core(at, slot):
        kc[slot] = send(at, at, s_c, r_c, slot, core_peer)

    def near_arrived(k):
        plane, slot = key_from[k]
        at = spot(plane * 2 + y, c)
        copy = pltpu.make_async_remote_copy(
            src_ref=at, dst_ref=at, send_sem=s_f.at[slot], recv_sem=r_z.at[slot],
            device_id={"sp": z_pair[0], "tp": tp}, device_id_type=MESH,
        )
        got("kz", copy)
        if k > 0:
            passed.append(copy)

            @pl.when(inner == 1)
            def _():
                copy.start()

        ky.append(send(at, at, s_y, r_y, k + 1, y_peer))
        to_core(at, 2 * k + 1)

    def far_arrived(k):
        got("ky", ky[k])
        to_core(spot((z if k == 0 else key_from[k - 1][0]) * 2 + 1 - y, c), 2 * k)

    def use(slot, owner):
        got("kc", kc[slot])
        turn_values(owner)
        attend(owner, 0, first)

    turn_values(sp)
    attend(sp, 0, first)
    far_arrived(0)
    near_arrived(0)
    use(0, z * 2 + 1 - y)
    for k in far:
        if k + 1 in far:
            near_arrived(k + 1)
        else:
            far_arrived(1)
        if k == far[-2]:
            pl.when(inner == 1)(give_pair)
            gy[-1, 0] = send(gu_ref.at[u], gu_all.at[rows_at(sp, depth), :], s_gy, r_gy, 0, y_peer)
        use(2 * k + 1, key_from[k][0] * 2 + y)
    for k in far:
        if k + 1 in far:
            far_arrived(k + 2)
        use(2 * k + 2, key_from[k][0] * 2 + 1 - y)

    def cols(t):
        return rows_at(t, own)

    def project(i):
        with jax.named_scope("proj"):
            parts = [
                (acc_s[i * heads + h] / sum_s[i * heads + h]).astype(BF16) for h in range(heads)
            ]
            whole = jnp.concatenate(parts, axis=0) if heads > 1 else parts[0]
            proj[rows_at(i, tile), :] = lax.dot_general(
                whole, w_ref[...], (((0,), (0,)), ((), ())), preferred_element_type=F32
            ).astype(BF16)

    near, to_x = {}, {}
    step = rows // 8
    small = tile // 4

    def give_core(t):
        at = pl.ds(t * tile, tile)
        for j in list(range(1, nx)) + [0]:
            near[t, j] = send(proj.at[at, cols(xs[j] * 2 + 1 - c)], from_core.at[j, at],
                              s1, r1, t * nx + j, core_peer)

    def give_x(t):
        for j in range(1, nx):
            got("near", near[t, j])

            @pl.loop(0, 4)
            def _(i):
                at = pl.ds(pl.multiple_of(t * tile + i * small, small), small)
                outgo[j - 1, at, :] = (
                    proj[at, cols(xs[j] * 2 + c)].astype(F32) + from_core[j, at, :].astype(F32)
                ).astype(BF16)

            at = pl.ds(t * tile, tile)
            to_x[t, j] = send(outgo.at[j - 1, at], from_x.at[j - 1, at], s2, r2,
                              t * (nx - 1) + j - 1, row_peers[j - 1])
        got("near", near[t, 0])

    def later(begin, end):
        @pl.loop(begin, end)
        def _(b):
            attend(b, first, tiles)

    def relay_gu(k, a, condition=None):
        at = gu_at(z_from[k] * 2 + y, k, a)
        if (k, a) not in gy:
            slot = (k + 1) * 2 + a
            gy[k, a] = pltpu.make_async_remote_copy(
                src_ref=at, dst_ref=at, send_sem=s_gy.at[slot], recv_sem=r_gy.at[slot],
                device_id={"sp": y_peer[0], "tp": y_peer[1]}, device_id_type=MESH,
            )
            sends.append(gy[k, a])

        def pass_on():
            got("gz" + str(k) + str(a), gz[k, a])
            gy[k, a].start()

        if condition is None:
            pass_on()
        else:
            pl.when(condition)(pass_on)

    def have_gu(k):
        for a in range(pieces(k)):
            got("gy" + str(k), gy[k, a])

    def relay_dn(k, condition=None):
        at = dn_all.at[:, rows_at(z_from[k] * 2 + y, wide)]
        if k not in dy:
            dy[k] = describe(at, at, s_dy, r_dy, k + 1, y_peer)

        def pass_on():
            got("dz" + str(k), dz[k])
            dy[k].start()

        if condition is None:
            pass_on()
        else:
            pl.when(condition)(pass_on)

    for t in range(first):
        project(t)
        give_core(t)
    relay_gu(0, 0, inner == 1)
    if tiles > first:
        later(0, 2)
    for t in range(first):
        give_x(t)
    for t in range(first, tiles):
        later(2, 2 * nz)
        project(t)
        give_core(t)
    relay_dn(0, inner == 1)
    relay_gu(0, 0, inner == 0)
    for t in range(first, tiles):
        give_x(t)

    ones = jnp.ones((8, own), F32)
    peers = [core_peer] + row_peers + across
    az, ax, ac, ar = [], {}, {}, {}

    def home(uu, tt, t):
        return normed_ref.at[rows_at(uu * tiles + t, tile), cols(tt)]

    def on_core(uu, tt, t, slot):
        at = home(uu, tt, t)
        ac[t, slot] = send(at, at, s_ac, r_ac, t * 2 * nx + slot, core_peer)

    def add_up(t):
        for j in range(1, nx):
            got("tox", to_x[t, j])
        at = pl.ds(t * tile, tile)
        with jax.named_scope("mid"):
            total = proj[at, cols(tp)].astype(F32) + from_core[0, at, :].astype(F32)
            for j in range(1, nx):
                total += from_x[j - 1, at, :].astype(F32)
            mid = res_ref[at, :].astype(F32) + total
            mid_ref[at, :] = mid
            made = (mid * gain_ref[:, cols(tp)]).astype(BF16)
            block[at, :] = made
            normed_ref[rows_at(u * tiles + t, tile), cols(tp)] = made
            squares[0, :, at] = lax.dot_general(
                ones, mid * mid, (((1,), (1,)), ((), ())),
                precision=lax.Precision.HIGHEST, preferred_element_type=F32,
            )
        az.append(send(block.at[at], home(u, tp, t), s_az, r_az, t, z_pair))
        for j in range(1, nx):
            ax[t, j] = send(block.at[at], home(u, tp, t), s_ax, r_ax, t * (nx - 1) + j - 1,
                            row_peers[j - 1])
        ac[t, 0] = send(block.at[at], home(u, tp, t), s_ac, r_ac, t * 2 * nx, core_peer)

    for t in range(tiles):
        add_up(t)
        if t == 0:
            for k in far[1:2]:
                relay_gu(k, 0, inner == 1)
    sq = [send(squares.at[0], squares.at[k + 1], s3, r3, k, peers[k]) for k in range(len(peers))]
    for k in far[1:]:
        dz[k].start()
    def gate_up(plane, uu, fresh=False):
        ks = rows_at(plane, 2 * depth)
        with jax.named_scope("gate_up"):
            @pl.loop(0, rows // 384)
            def _(i):
                at = pl.ds(pl.multiple_of(uu * rows + i * 384, 384), 384)
                term = jnp.dot(normed_ref[at, ks], gu_all[ks, :], preferred_element_type=F32)
                gu_acc[at, :] = term if fresh else gu_acc[at, :] + term

    for t in range(tiles):
        for j in range(1, nx):
            got("ax", ax[t, j])
            on_core(u, back[j] * 2 + c, t, j)
    for t in range(tiles):
        for j in range(nx):
            got("ac", ac[t, j])
    for k in far[1:2]:
        relay_gu(k, 0, inner == 0)
    relay_dn(0, inner == 0)
    have_gu(-1)
    gate_up(z, u, True)
    for k in far[1:2]:
        relay_gu(k, 1)
    have_gu(0)
    gate_up(z_from[0], u)
    for k in far[2:3]:
        relay_gu(k, 0)
    for t in range(tiles):
        if t == tiles - 1:
            for k in far[2:3]:
                relay_gu(k, 1)
        got("az", az[t])
        there = home(1 - u, tp, t)
        for j in range(1, nx):
            ar[t, j] = send(there, there, s_ar, r_ar, t * (nx - 1) + j - 1, row_peers[j - 1])
        on_core(1 - u, tp, t, nx)
    for copy in sq:
        got("sq", copy)
    with jax.named_scope("norm"):
        square = squares[0]
        for k in range(len(peers)):
            square += squares[k + 1]
        ratio[u] = lax.rsqrt(square / (n_tp * own) + eps)
    ratio_z = send(ratio.at[u], ratio.at[u], s_rz, r_rz, 0, z_pair)
    for k in far[3:]:
        for a in range(2):
            relay_gu(k, a)
    for k in far[1:2]:
        relay_dn(k, inner == 0)
    for t in range(tiles):
        for j in range(1, nx):
            got("ar", ar[t, j])
            on_core(1 - u, back[j] * 2 + c, t, nx + j)
    for k in far[1:2]:
        relay_dn(k, inner == 1)
    for k in far[2:3]:
        relay_dn(k, inner == 0)
    for t in range(tiles):
        for j in range(nx, 2 * nx):
            got("ac", ac[t, j])
    gate_up(z, 1 - u, True)
    gate_up(z_from[0], 1 - u)
    for k in far[2:3]:
        relay_dn(k, inner == 1)
    for k in far[3:]:
        relay_dn(k)
    for k in far[1:]:
        have_gu(k)
        gate_up(z_from[k], 1 - u)
        gate_up(z_from[k], u)

    got("ratio", ratio_z)
    for uu in range(2):
        column[pl.ds(uu * rows, rows), :] = ratio[uu].T
    with jax.named_scope("hidden"):
        for uu in range(2):
            @pl.loop(0, rows // 128)
            def _(i):
                at = pl.ds(pl.multiple_of(uu * rows + i * 128, 128), 128)
                scale = column[at, 0:1]
                gate = gu_acc[at, :units] * scale
                hidden[at, :] = (
                    gate / (1.0 + jnp.exp(-gate)) * (gu_acc[at, units:] * scale)
                ).astype(BF16)

    for k in [-1] + list(far):
        got("dy", dy[k])
    top, low = pl.ds(0, half), pl.ds(half, half)
    x_peers = [(sp, xs[j] * 2 + c) for j in range(nx)]
    every = [(1 - u, xs[j]) for j in range(nx)] + [(u, xs[j]) for j in range(1, nx)] + [(u, x)]
    turns = list(range(1, 2 * nx - 1)) + [0, 2 * nx - 1]
    side, to_z, to_x, again = {}, {}, {}, []

    def down(k):
        uu, xx = every[k]
        ks = rows_at(xx, 2 * own)
        with jax.named_scope("down"):
            @pl.loop(0, rows // 384)
            def _(i):
                at = pl.ds(pl.multiple_of(uu * rows + i * 384, 384), 384)
                terms[at, ks] = jnp.dot(
                    hidden[at, :], dn_all[:, ks], preferred_element_type=F32
                ).astype(BF16)

        side[k] = send(terms.at[rows_at(uu, rows), cols(xx * 2 + 1 - c)], d_core.at[k],
                       e1, f1, k, core_peer)

    def forward(k):
        uu, xx = every[k]
        got("side", side[k])

        @pl.loop(0, 8)
        def _(i):
            at = rows_at(i, step)
            here = pl.ds(pl.multiple_of(uu * rows + i * step, step), step)
            d_out[k, at, :] = (
                terms[here, cols(xx * 2 + c)].astype(F32) + d_core[k, at, :].astype(F32)
            ).astype(BF16)

        if k < nx:
            to_z[k] = send(d_out.at[k, top], d_y.at[k], e2, f2, k, z_pair)
        j = k if k < nx else k - nx + 1
        if j > 0:
            slot = 2 * (j - 1) + (1 if k < nx else 0)
            to_x[slot] = send(d_out.at[k, low], d_x.at[slot], e3, f3, slot, x_peers[j])

    for i, k in enumerate(turns):
        down(k)
        if i > 0:
            forward(turns[i - 1])
    for j in range(1, nx):
        got("to_z", to_z[j])

        @pl.loop(0, 4)
        def _(i):
            at = rows_at(i, step)
            relay[j, at, :] = (
                d_out[nx + j - 1, at, :].astype(F32) + d_y[j, at, :].astype(F32)
            ).astype(BF16)

        again.append(send(relay.at[j], last_x.at[j - 1], e4, f4, j - 1, x_peers[j]))
    for j in range(1, nx):
        got("to_x", to_x[2 * j - 1])

    @pl.loop(0, 4)
    def _(i):
        at = rows_at(i, step)
        here = pl.ds(pl.multiple_of(half + i * step, step), step)
        total = d_out[0, here, :].astype(F32)
        for j in range(1, nx):
            total += d_x[2 * j - 1, at, :].astype(F32)
        relay[0, at, :] = total.astype(BF16)

    again.append(send(relay.at[0], last_y, e5, f5, 0, z_pair))
    got("side", side[2 * nx - 1])
    got("to_z", to_z[0])
    for j in range(1, nx):
        got("to_x", to_x[2 * j - 2])
    for copy in again:
        got("again", copy)

    with jax.named_scope("final"):
        @pl.loop(0, 4)
        def _(i):
            at = rows_at(i, step)
            for part in range(2):
                to = pl.ds(pl.multiple_of(part * half + i * step, step), step)
                here = pl.ds(pl.multiple_of(u * rows + part * half + i * step, step), step)
                total = terms[here, cols(tp)].astype(F32)
                total += d_core[2 * nx - 1, to, :].astype(F32)
                total += (d_y[0, at, :] if part == 0 else last_y[at, :]).astype(F32)
                for j in range(1, nx):
                    total += (last_x[j - 1, at, :] if part == 0
                              else d_x[2 * j - 2, at, :]).astype(F32)
                out_ref[to, :] = (mid_ref[to, :] + 0.5 * total).astype(BF16)

    with jax.named_scope("w_sends"):
        @pl.when(inner == 1)
        def _():
            for copy in passed:
                copy.wait_send()

        for copy in sends:
            copy.wait_send()


def layer(q, k, v, q_gain, k_gain, w, res, gain, gate, up, dn, n_sp, n_tp):
    nz, nx = n_sp // 2, n_tp // 2
    rows, own = res.shape
    heads = q.shape[1] // HEAD_SIZE
    tile = 256 if rows % 256 == 0 else rows
    tiles = rows // tile
    count = heads * tiles
    width = n_tp * own
    depth, twice = gate.shape
    wide = dn.shape[2]
    dma = pltpu.SemaphoreType.DMA
    n = 2 * nx
    vm = pl.BlockSpec(memory_space=pltpu.VMEM)

    def two(k):
        return [dma((k,)), dma((k,))]

    def bf(*shape):
        return pltpu.VMEM(shape, BF16)

    def fl(*shape):
        return pltpu.VMEM(shape, F32)

    return pl.pallas_call(
        functools.partial(layer_kernel, nz, nx, heads),
        out_shape=jax.ShapeDtypeStruct((rows, own), BF16),
        in_specs=[vm] * 15,
        out_specs=vm,
        scratch_shapes=[
            bf(rows, heads * HEAD_SIZE), bf(rows, 2 * HEAD_SIZE),
            bf(n_sp * rows, 2 * HEAD_SIZE), bf(n_sp, HEAD_SIZE, rows),
            fl(count, 1, tile), fl(count, 1, tile), fl(count, HEAD_SIZE, tile),
            bf(rows, width), bf(nx, rows, own), bf(nx - 1, rows, own), bf(nx - 1, rows, own),
            fl(n, 8, rows), bf(rows, own), fl(rows, own), bf(2 * rows, width),
            bf(2, depth, twice), bf(n_sp * depth, twice), bf(dn.shape[1], n_sp * wide),
            fl(2 * rows, twice), bf(2 * rows, twice // 2), fl(2, 8, rows), fl(2 * rows, 8), bf(2 * rows, width),
            bf(n, rows, own), bf(n - 1, rows, own), bf(nx, rows // 2, own),
            bf(n - 2, rows // 2, own), bf(nx, rows // 2, own), bf(nx - 1, rows // 2, own),
            bf(rows // 2, own),
        ] + two(nz - 1) + [dma((nz - 1,))] + two(nz) + two(2 * nz - 1)
        + two(tiles * nx) + two(tiles * (nx - 1)) + two(n - 1)
        + two(tiles * (nx - 1)) + two(tiles) + two(tiles * (nx - 1)) + two(tiles * 2 * nx)
        + two(1) + two(2 * nz) + two(2 * nz) + two(nz - 1) + two(nz)
        + two(n) + two(nx) + two(n - 2) + two(nx - 1) + two(1),
        compiler_params=pltpu.CompilerParams(
            collective_id=0, has_side_effects=True, vmem_limit_bytes=VMEM_LIMIT
        ),
        name="layer",
    )(q, k, v, q_gain, k_gain, w, res, gain, gate, up, dn, *rotary_tables(n_sp * rows))


def on_device(n_sp, n_tp, residual_in, queries, keys, values, query_gain, key_norm_gain,
              out_weight, mlp_gain, gate_weight, up_weight, down_weight):
    down = down_weight.reshape(2, down_weight.shape[0] // 2, down_weight.shape[1])
    return layer(
        queries, keys, values, query_gain[None, :], key_norm_gain[None, :], out_weight,
        residual_in, mlp_gain[None, :], gate_weight, up_weight, down, n_sp, n_tp,
    )


def solution(mesh):
    in_specs = (
        P("sp", "tp"),
        P("sp", "tp"),
        P("sp", None),
        P("sp", None),
        P(),
        P(),
        P("tp", None),
        P(),
        P("sp", "tp"),
        P("sp", "tp"),
        P("tp", "sp"),
    )
    out_specs = P("sp", "tp")
    return jax.shard_map(
        functools.partial(on_device, mesh.shape["sp"], mesh.shape["tp"]),
        mesh=mesh, in_specs=in_specs, out_specs=out_specs, check_vma=False,
    )
```

time: 203 us -> 171 us (0.84)
  the two profiles are of different devices: /device:TPU:16 before, /device:TPU:0 now
where the time goes in v3:
time: 171 us
  Pallas kernels  169 us (99%)
  local copies, waits for them, and re-layouts  2.06 us (1%)
    pallas_call x1, Pallas kernels, layer(): pl.pallas_call(functools.partial(layer_kernel, nz, nx, heads), out_shape=...  169 us

profile of v3, /device:TPU:0, one launch (start us, length us, event | category | flops | bytes accessed | tf_op | source)
XLA Modules:
  0.0 171.1 jit_solution(13894858571199707496)
XLA Ops:
  0.0 169.0 %layer.1 = bf16[768,512]{1,0:T(8,128)(2,1)} custom-call(bf16[768,256]{1,0:T(8,128)(2,1)} %q_in.1, bf16[768,256]{1,0:T(8,128)(2,1)} %k_in.1, bf16[768,256]{1,0:T(8,128)(2,1)} %v_in.1, f32[1,128]{1,0:T(1,128)} %bitcast.6, f32[1,128]{1,0:T(1,128)} %bitcast.7, bf16[256,2048]{1,0:T(8,128)(2,1)} %w_ref.1, bf16[768,512]{1,0:T(8,128)(2,1)} %res_ref.1, ...), custom_call_target="tpu_custom_call" | custom-call | tf_op jit(solution)/shard_map/layer/pallas_call | solution.py:666
  169.0 2.1 %copy.17 = bf16[768,512]{1,0:T(8,128)(2,1)} copy(bf16[768,512]{1,0:T(8,128)(2,1)} %layer.1) | data formatting | bytes 1572864

commit v4 on v3

--- a/solution.py
+++ b/solution.py
@@ -197,11 +197,17 @@
             gz[k, a] = describe(gu_ref.at[lax.rem(z_to[k], 2), pl.ds(a * size, size)],
                                 gu_at(sp, k, a), s_gz, r_gz, slots_z[k] * 2 + a, z_peers[k])
 
+    def dn_at(owner, k, a):
+        size = units // pieces(k)
+        return dn_all.at[pl.ds(a * size, size), rows_at(owner, wide)]
+
     def give_dn(k):
-        dz[k] = describe(dn_ref.at[lax.rem(z_to[k], 2)], dn_all.at[:, rows_at(sp, wide)],
-                         s_dz, r_dz, slots_z[k], z_peers[k])
-
-    dy[-1] = send(dn_ref.at[u], dn_all.at[:, rows_at(sp, wide)], s_dy, r_dy, 0, y_peer)
+        for a in range(pieces(k)):
+            size = units // pieces(k)
+            dz[k, a] = describe(dn_ref.at[lax.rem(z_to[k], 2), pl.ds(a * size, size)],
+                                dn_at(sp, k, a), s_dz, r_dz, slots_z[k] * 2 + a, z_peers[k])
+
+    dy[-1, 0] = send(dn_ref.at[u], dn_all.at[:, rows_at(sp, wide)], s_dy, r_dy, 0, y_peer)
     for k in far:
         give_gu(k)
         give_dn(k)
@@ -210,7 +216,7 @@
         gz[0, 0].start()
 
     pl.when(inner == 0)(give_pair)
-    dz[0].start()
+    dz[0, 0].start()
     for k in far[1:]:
         for a in range(pieces(k)):
             gz[k, a].start()
@@ -382,13 +388,15 @@
             got("gy" + str(k), gy[k, a])
 
     def relay_dn(k, condition=None):
-        at = dn_all.at[:, rows_at(z_from[k] * 2 + y, wide)]
-        if k not in dy:
-            dy[k] = describe(at, at, s_dy, r_dy, k + 1, y_peer)
+        for a in range(pieces(k)):
+            at = dn_at(z_from[k] * 2 + y, k, a)
+            if (k, a) not in dy:
+                dy[k, a] = describe(at, at, s_dy, r_dy, (k + 1) * 2 + a, y_peer)
 
         def pass_on():
-            got("dz" + str(k), dz[k])
-            dy[k].start()
+            for a in range(pieces(k)):
+                got("dz" + str(k), dz[k, a])
+                dy[k, a].start()
 
         if condition is None:
             pass_on()
@@ -399,6 +407,7 @@
         project(t)
         give_core(t)
     relay_gu(0, 0, inner == 1)
+    relay_dn(0, inner == 0)
     if tiles > first:
         later(0, 2)
     for t in range(first):
@@ -453,7 +462,8 @@
                 relay_gu(k, 0, inner == 1)
     sq = [send(squares.at[0], squares.at[k + 1], s3, r3, k, peers[k]) for k in range(len(peers))]
     for k in far[1:]:
-        dz[k].start()
+        for a in range(2):
+            dz[k, a].start()
     def gate_up(plane, uu, fresh=False):
         ks = rows_at(plane, 2 * depth)
         with jax.named_scope("gate_up"):
@@ -463,6 +473,8 @@
                 term = jnp.dot(normed_ref[at, ks], gu_all[ks, :], preferred_element_type=F32)
                 gu_acc[at, :] = term if fresh else gu_acc[at, :] + term
 
+    for k in far[1:2]:
+        relay_gu(k, 0, inner == 0)
     for t in range(tiles):
         for j in range(1, nx):
             got("ax", ax[t, j])
@@ -470,9 +482,6 @@
     for t in range(tiles):
         for j in range(nx):
             got("ac", ac[t, j])
-    for k in far[1:2]:
-        relay_gu(k, 0, inner == 0)
-    relay_dn(0, inner == 0)
     have_gu(-1)
     gate_up(z, u, True)
     for k in far[1:2]:
@@ -501,16 +510,12 @@
     for k in far[3:]:
         for a in range(2):
             relay_gu(k, a)
-    for k in far[1:2]:
-        relay_dn(k, inner == 0)
     for t in range(tiles):
         for j in range(1, nx):
             got("ar", ar[t, j])
             on_core(1 - u, back[j] * 2 + c, t, nx + j)
     for k in far[1:2]:
         relay_dn(k, inner == 1)
-    for k in far[2:3]:
-        relay_dn(k, inner == 0)
     for t in range(tiles):
         for j in range(nx, 2 * nx):
             got("ac", ac[t, j])
@@ -521,6 +526,9 @@
     for k in far[3:]:
         relay_dn(k)
     for k in far[1:]:
+        if k == 2:
+            relay_dn(1, inner == 0)
+            relay_dn(2, inner == 0)
         have_gu(k)
         gate_up(z_from[k], 1 - u)
         gate_up(z_from[k], u)
@@ -539,79 +547,94 @@
                     gate / (1.0 + jnp.exp(-gate)) * (gu_acc[at, units:] * scale)
                 ).astype(BF16)
 
-    for k in [-1] + list(far):
-        got("dy", dy[k])
     top, low = pl.ds(0, half), pl.ds(half, half)
     x_peers = [(sp, xs[j] * 2 + c) for j in range(nx)]
     every = [(1 - u, xs[j]) for j in range(nx)] + [(u, xs[j]) for j in range(1, nx)] + [(u, x)]
     turns = list(range(1, 2 * nx - 1)) + [0, 2 * nx - 1]
     side, to_z, to_x, again = {}, {}, {}, []
-
-    def down(k):
+    which = [y, 1 - y]
+
+    def sub(v):
+        return rows_at(which[v], wide)
+
+    def block_at(t, v):
+        return rows_at(t * 2 + which[v], wide)
+
+    def down(k, v):
         uu, xx = every[k]
-        ks = rows_at(xx, 2 * own)
+        at = rows_at(uu, rows)
         with jax.named_scope("down"):
-            @pl.loop(0, rows // 384)
-            def _(i):
-                at = pl.ds(pl.multiple_of(uu * rows + i * 384, 384), 384)
+            for core in range(2):
+                ks = block_at(xx * 2 + core, v)
                 terms[at, ks] = jnp.dot(
                     hidden[at, :], dn_all[:, ks], preferred_element_type=F32
                 ).astype(BF16)
-
-        side[k] = send(terms.at[rows_at(uu, rows), cols(xx * 2 + 1 - c)], d_core.at[k],
-                       e1, f1, k, core_peer)
-
-    def forward(k):
+        side[k, v] = send(terms.at[at, block_at(xx * 2 + 1 - c, v)], d_core.at[k, :, sub(v)],
+                          e1, f1, 2 * k + v, core_peer)
+
+    def forward(k, v):
         uu, xx = every[k]
-        got("side", side[k])
-
-        @pl.loop(0, 8)
+        got("side", side[k, v])
+
+        @pl.loop(0, 4)
         def _(i):
-            at = rows_at(i, step)
-            here = pl.ds(pl.multiple_of(uu * rows + i * step, step), step)
-            d_out[k, at, :] = (
-                terms[here, cols(xx * 2 + c)].astype(F32) + d_core[k, at, :].astype(F32)
+            at = rows_at(i, 2 * step)
+            here = pl.ds(pl.multiple_of(uu * rows + i * 2 * step, 2 * step), 2 * step)
+            d_out[k, at, sub(v)] = (
+                terms[here, block_at(xx * 2 + c, v)].astype(F32)
+                + d_core[k, at, sub(v)].astype(F32)
             ).astype(BF16)
 
         if k < nx:
-            to_z[k] = send(d_out.at[k, top], d_y.at[k], e2, f2, k, z_pair)
+            to_z[k, v] = send(d_out.at[k, top, sub(v)], d_y.at[k, :, sub(v)],
+                              e2, f2, 2 * k + v, z_pair)
         j = k if k < nx else k - nx + 1
         if j > 0:
             slot = 2 * (j - 1) + (1 if k < nx else 0)
-            to_x[slot] = send(d_out.at[k, low], d_x.at[slot], e3, f3, slot, x_peers[j])
-
-    for i, k in enumerate(turns):
-        down(k)
-        if i > 0:
-            forward(turns[i - 1])
-    for j in range(1, nx):
-        got("to_z", to_z[j])
+            to_x[slot, v] = send(d_out.at[k, low, sub(v)], d_x.at[slot, :, sub(v)],
+                                 e3, f3, 2 * slot + v, x_peers[j])
+
+    for v in range(2):
+        if v == 1:
+            for k in [-1] + list(far):
+                for a in range(pieces(k)):
+                    got("dy", dy[k, a])
+        for i, k in enumerate(turns):
+            down(k, v)
+            if i > 0:
+                forward(turns[i - 1], v)
+
+    for v in range(2):
+        for j in range(1, nx):
+            got("to_z", to_z[j, v])
+
+            @pl.loop(0, 4)
+            def _(i):
+                at = rows_at(i, step)
+                relay[j, at, sub(v)] = (
+                    d_out[nx + j - 1, at, sub(v)].astype(F32) + d_y[j, at, sub(v)].astype(F32)
+                ).astype(BF16)
+
+            again.append(send(relay.at[j, :, sub(v)], last_x.at[j - 1, :, sub(v)],
+                              e4, f4, 2 * (j - 1) + v, x_peers[j]))
+        for j in range(1, nx):
+            got("to_x", to_x[2 * j - 1, v])
 
         @pl.loop(0, 4)
         def _(i):
             at = rows_at(i, step)
-            relay[j, at, :] = (
-                d_out[nx + j - 1, at, :].astype(F32) + d_y[j, at, :].astype(F32)
-            ).astype(BF16)
-
-        again.append(send(relay.at[j], last_x.at[j - 1], e4, f4, j - 1, x_peers[j]))
-    for j in range(1, nx):
-        got("to_x", to_x[2 * j - 1])
-
-    @pl.loop(0, 4)
-    def _(i):
-        at = rows_at(i, step)
-        here = pl.ds(pl.multiple_of(half + i * step, step), step)
-        total = d_out[0, here, :].astype(F32)
-        for j in range(1, nx):
-            total += d_x[2 * j - 1, at, :].astype(F32)
-        relay[0, at, :] = total.astype(BF16)
-
-    again.append(send(relay.at[0], last_y, e5, f5, 0, z_pair))
-    got("side", side[2 * nx - 1])
-    got("to_z", to_z[0])
-    for j in range(1, nx):
-        got("to_x", to_x[2 * j - 2])
+            here = pl.ds(pl.multiple_of(half + i * step, step), step)
+            total = d_out[0, here, sub(v)].astype(F32)
+            for j in range(1, nx):
+                total += d_x[2 * j - 1, at, sub(v)].astype(F32)
+            relay[0, at, sub(v)] = total.astype(BF16)
+
+        again.append(send(relay.at[0, :, sub(v)], last_y.at[:, sub(v)], e5, f5, v, z_pair))
+    for v in range(2):
+        got("side", side[2 * nx - 1, v])
+        got("to_z", to_z[0, v])
+        for j in range(1, nx):
+            got("to_x", to_x[2 * j - 2, v])
     for copy in again:
         got("again", copy)
 
@@ -682,8 +705,8 @@
         ] + two(nz - 1) + [dma((nz - 1,))] + two(nz) + two(2 * nz - 1)
         + two(tiles * nx) + two(tiles * (nx - 1)) + two(n - 1)
         + two(tiles * (nx - 1)) + two(tiles) + two(tiles * (nx - 1)) + two(tiles * 2 * nx)
-        + two(1) + two(2 * nz) + two(2 * nz) + two(nz - 1) + two(nz)
-        + two(n) + two(nx) + two(n - 2) + two(nx - 1) + two(1),
+        + two(1) + two(2 * nz) + two(2 * nz) + two(2 * nz) + two(2 * nz)
+        + two(2 * n) + two(2 * nx) + two(2 * n - 4) + two(2 * nx - 2) + two(2),
         compiler_params=pltpu.CompilerParams(
             collective_id=0, has_side_effects=True, vmem_limit_bytes=VMEM_LIMIT
         ),

time: 171 us -> 153 us (0.89)
  Pallas kernels: 169 us -> 150 us
    pallas_call x1, Pallas kernels: 169 us -> 150 us  [layer(): pl.pallas_call(functools.partial(layer_kernel, nz, nx, heads), out_shape=...]
where the time goes in v4:
time: 153 us
  Pallas kernels  150 us (98%)
  local copies, waits for them, and re-layouts  2.06 us (1%)
    pallas_call x1, Pallas kernels, layer(): pl.pallas_call(functools.partial(layer_kernel, nz, nx, heads), out_shape=...  150 us

profile of v4, /device:TPU:0, one launch (start us, length us, event | category | flops | bytes accessed | tf_op | source)
XLA Modules:
  0.0 152.6 jit_solution(639296479308757563)
XLA Ops:
  0.0 150.5 %layer.1 = bf16[768,512]{1,0:T(8,128)(2,1)} custom-call(bf16[768,256]{1,0:T(8,128)(2,1)} %q_in.1, bf16[768,256]{1,0:T(8,128)(2,1)} %k_in.1, bf16[768,256]{1,0:T(8,128)(2,1)} %v_in.1, f32[1,128]{1,0:T(1,128)} %bitcast.6, f32[1,128]{1,0:T(1,128)} %bitcast.7, bf16[256,2048]{1,0:T(8,128)(2,1)} %w_ref.1, bf16[768,512]{1,0:T(8,128)(2,1)} %res_ref.1, ...), custom_call_target="tpu_custom_call" | custom-call | tf_op jit(solution)/shard_map/layer/pallas_call | solution.py:689
  150.5 2.1 %copy.17 = bf16[768,512]{1,0:T(8,128)(2,1)} copy(bf16[768,512]{1,0:T(8,128)(2,1)} %layer.1) | data formatting | bytes 1572864

commit v5 on v4

--- a/solution.py
+++ b/solution.py
@@ -536,8 +536,8 @@
     got("ratio", ratio_z)
     for uu in range(2):
         column[pl.ds(uu * rows, rows), :] = ratio[uu].T
-    with jax.named_scope("hidden"):
-        for uu in range(2):
+    def activate(uu):
+        with jax.named_scope("hidden"):
             @pl.loop(0, rows // 128)
             def _(i):
                 at = pl.ds(pl.multiple_of(uu * rows + i * 128, 128), 128)
@@ -547,6 +547,7 @@
                     gate / (1.0 + jnp.exp(-gate)) * (gu_acc[at, units:] * scale)
                 ).astype(BF16)
 
+    activate(1 - u)
     top, low = pl.ds(0, half), pl.ds(half, half)
     x_peers = [(sp, xs[j] * 2 + c) for j in range(nx)]
     every = [(1 - u, xs[j]) for j in range(nx)] + [(u, xs[j]) for j in range(1, nx)] + [(u, x)]
@@ -601,10 +602,11 @@
                     got("dy", dy[k, a])
         for i, k in enumerate(turns):
             down(k, v)
+            if i == 0 and v == 0:
+                activate(u)
             if i > 0:
                 forward(turns[i - 1], v)
 
-    for v in range(2):
         for j in range(1, nx):
             got("to_z", to_z[j, v])
 

time: 153 us -> 151 us (0.987)
  no operation moved by 1% of the time
where the time goes in v5:
time: 151 us
  Pallas kernels  149 us (99%)
  local copies, waits for them, and re-layouts  2.06 us (1%)
    pallas_call x1, Pallas kernels, layer(): pl.pallas_call(functools.partial(layer_kernel, nz, nx, heads), out_shape=...  149 us

profile of v5, /device:TPU:0, one launch (start us, length us, event | category | flops | bytes accessed | tf_op | source)
XLA Modules:
  0.0 151.3 jit_solution(9796457671677440393)
XLA Ops:
  0.0 149.2 %layer.1 = bf16[768,512]{1,0:T(8,128)(2,1)} custom-call(bf16[768,256]{1,0:T(8,128)(2,1)} %q_in.1, bf16[768,256]{1,0:T(8,128)(2,1)} %k_in.1, bf16[768,256]{1,0:T(8,128)(2,1)} %v_in.1, f32[1,128]{1,0:T(1,128)} %bitcast.6, f32[1,128]{1,0:T(1,128)} %bitcast.7, bf16[256,2048]{1,0:T(8,128)(2,1)} %w_ref.1, bf16[768,512]{1,0:T(8,128)(2,1)} %res_ref.1, ...), custom_call_target="tpu_custom_call" | custom-call | tf_op jit(solution)/shard_map/layer/pallas_call | solution.py:691
  149.2 2.1 %copy.17 = bf16[768,512]{1,0:T(8,128)(2,1)} copy(bf16[768,512]{1,0:T(8,128)(2,1)} %layer.1) | data formatting | bytes 1572864
